TPU v7x, 256 devices: a whole 4x4x8 slice. The times are simulated.
256 devices in a mesh: sp: 16 (over y, x), dp: 16 (over z, core).
Axes of the slice: x: 4, y: 4, z: 8, core: 2. Of those that a mesh axis runs over, the one named last changes fastest.
Arguments:
- tokens: bfloat16 [16, 2560, 2048], P('dp', 'sp'), may hold values from -42 to 42
- query_weight: bfloat16 [2048, 1024], P('dp'), may hold values from -1 to 1
- key_weight: bfloat16 [2048, 1024], P('dp'), may hold values from -1 to 1
- values: bfloat16 [16, 2560, 1024], P('dp', 'sp'), may hold values from -6 to 6
- lambdas: float32 [16], replicated, may hold values from 0.3 to 0.8
- out_grad: bfloat16 [16, 2560, 1024], P('dp', 'sp'), may hold values from -6 to 6
Outputs:
- tokens_grad: bfloat16 [16, 2560, 2048], P('dp', 'sp')
- values_grad: bfloat16 [16, 2560, 1024], P('dp', 'sp')
- query_weight_grad: float32 [2048, 1024], P('dp')
- key_weight_grad: float32 [2048, 1024], P('dp')
All inputs are finite; a program needn't handle non-finite values.
Results may differ from a plain program's by a relative error of at most 0.029.
The roundings to bfloat16 on the way count: a program that leaves them out, or rounds other values in their place, can miss the bound.
Values may be sent and summed in bfloat16 or wider, within the bound.
A program may use at most 128 MiB of HBM per device.

v0:
```python
import math

import jax
import jax.numpy as jnp
from jax import lax
from jax.sharding import PartitionSpec as P

DQK = 32


NORM_EPS = 0.1
THETA = 10000.0


def side_by_side(arrays, axis, dim, along):
    ends, at = ([], 0)
    for a in arrays[:-1]:
        at += a.shape[along]
        ends.append(at)
    both = jnp.concatenate(arrays, axis=along)
    return tuple(jnp.split(lax.all_gather(both, axis, axis=dim, tiled=True), ends, axis=along))


def side_by_side_2(arrays, axis, split_dim, concat_dim, along):
    both = jnp.concatenate(arrays, axis=along)
    whole, at, done = (
        lax.all_to_all(both, axis, split_axis=split_dim, concat_axis=concat_dim, tiled=True),
        0,
        [],
    )
    for a in arrays:
        done.append(lax.slice_in_dim(whole, at, at + a.shape[along], axis=along))
        at += a.shape[along]
    return tuple(done)


def rotation_tables(positions, vec_width):
    half_width = vec_width // 2
    freqs = jnp.exp(-math.log(THETA) * jnp.arange(half_width, dtype=jnp.float32) / half_width)
    angles = positions.astype(jnp.float32)[:, None] * freqs[None, :]
    return (jnp.cos(angles), jnp.sin(angles))


def rotate(field, cosine, sine_table, vec_width, sign_value):
    full_shape = field.shape
    grouped = field.reshape(full_shape[:-1] + (full_shape[-1] // vec_width, 2, vec_width // 2))
    first_half = grouped[..., 0, :]
    second_half = grouped[..., 1, :]
    cos_cols = cosine[:, None, :]
    sin_cols = sign_value * sine_table[:, None, :]
    turned = jnp.stack(
        [
            first_half * cos_cols - second_half * sin_cols,
            second_half * cos_cols + first_half * sin_cols,
        ],
        axis=-2,
    )
    return turned.reshape(full_shape)


def pair_product(pattern, first_op, second_op):
    return jnp.einsum(pattern, first_op, second_op, preferred_element_type=jnp.float32)


def head_backward(query_rot, key_rot, value_rows, grad_rows, lambda_here, cosine, sine_table):
    seq_length = query_rot.shape[0]
    head_count = lambda_here.shape[0]
    qk_width = query_rot.shape[1] // (2 * head_count)
    value_width = value_rows.shape[1] // head_count
    block_rows = math.gcd(seq_length, 512)
    block_count = seq_length // block_rows
    inv_root = 1.0 / math.sqrt(qk_width)
    query_split = query_rot.reshape(block_count, block_rows, head_count, 2, qk_width)
    key_split = key_rot.reshape(seq_length, head_count, 2, qk_width)
    value_split = value_rows.reshape(seq_length, head_count, value_width)
    grad_split = grad_rows.reshape(block_count, block_rows, head_count, value_width)
    lambda_col = lambda_here[:, None, None]
    key_positions = jnp.arange(seq_length, dtype=jnp.int32)

    def block_step(carried, inputs):
        key_sum, value_sum = carried
        query_part, grad_part, block_start = inputs
        scores = pair_product("qhmd,khmd->hmqk", query_part, key_split) * inv_root
        query_positions = block_start + jnp.arange(block_rows, dtype=jnp.int32)
        causal_mask = key_positions[None, :] <= query_positions[:, None]
        scores = jnp.where(causal_mask, scores, -jnp.inf)
        row_max = jnp.max(scores, axis=-1, keepdims=True)
        exp_scores = jnp.exp(scores - row_max)
        prob_maps = exp_scores / jnp.sum(exp_scores, axis=-1, keepdims=True)
        weights = (prob_maps[:, 0] - lambda_col * prob_maps[:, 1]).astype(jnp.bfloat16)
        mixed_out = pair_product("hqk,khe->qhe", weights, value_split)
        norm_scale = lax.rsqrt(jnp.mean(mixed_out * mixed_out, axis=-1, keepdims=True) + NORM_EPS)
        grad_float = grad_part.astype(jnp.float32)
        mixed_grad = (
            norm_scale * grad_float
            - norm_scale
            * norm_scale
            * norm_scale
            * mixed_out
            * jnp.mean(grad_float * mixed_out, axis=-1, keepdims=True)
        ).astype(jnp.bfloat16)
        weight_grad = pair_product("qhe,khe->hqk", mixed_grad, value_split)
        value_sum = value_sum + pair_product("hqk,qhe->khe", weights, mixed_grad)
        first_grad = prob_maps[:, 0] * (
            weight_grad - jnp.sum(weight_grad * prob_maps[:, 0], axis=-1, keepdims=True)
        )
        second_grad = (
            -lambda_col
            * prob_maps[:, 1]
            * (weight_grad - jnp.sum(weight_grad * prob_maps[:, 1], axis=-1, keepdims=True))
        )
        score_grad = (jnp.stack([first_grad, second_grad], axis=1) * inv_root).astype(jnp.bfloat16)
        query_grad = pair_product("hmqk,khmd->qhmd", score_grad, key_split)
        key_sum = key_sum + pair_product("hmqk,qhmd->khmd", score_grad, query_part)
        return ((key_sum, value_sum), query_grad)

    zero_init = (
        jnp.zeros((seq_length, head_count, 2, qk_width), jnp.float32),
        jnp.zeros((seq_length, head_count, value_width), jnp.float32),
    )
    block_starts = jnp.arange(block_count, dtype=jnp.int32) * block_rows
    (key_sum, value_sum), query_blocks = lax.scan(
        block_step, zero_init, (query_split, grad_split, block_starts)
    )
    query_turned = query_blocks.reshape(seq_length, head_count * 2 * qk_width)
    key_turned = key_sum.reshape(seq_length, head_count * 2 * qk_width)
    query_back = rotate(query_turned, cosine, sine_table, qk_width, -1.0).astype(jnp.bfloat16)
    key_back = rotate(key_turned, cosine, sine_table, qk_width, -1.0).astype(jnp.bfloat16)
    values_back = value_sum.reshape(seq_length, head_count * value_width).astype(jnp.bfloat16)
    return (query_back, key_back, values_back)


def body(tokens, query_weight, key_weight, values, lambdas, out_grad):
    sp_count = lax.axis_size("sp")
    dp_count = lax.axis_size("dp")
    tok_rows = tokens.shape[1]
    head_total = lambdas.shape[0]
    token_block = tokens[0]
    positions = lax.axis_index("sp") * tok_rows + jnp.arange(tok_rows, dtype=jnp.int32)
    cosine, sine_table = rotation_tables(positions, DQK)
    whole_query, whole_key = side_by_side((query_weight, key_weight), "dp", 0, 1)
    query_raw = jnp.dot(token_block, whole_query, preferred_element_type=jnp.float32)
    key_raw = jnp.dot(token_block, whole_key, preferred_element_type=jnp.float32)
    query_rot = rotate(query_raw, cosine, sine_table, DQK, 1.0).reshape(
        tok_rows, head_total, 2 * DQK
    )
    key_rot = rotate(key_raw, cosine, sine_table, DQK, 1.0).reshape(tok_rows, head_total, 2 * DQK)
    packed = (
        jnp.stack((query_rot, key_rot), axis=2)
        .reshape(1, tok_rows, head_total * 4 * DQK)
        .astype(jnp.bfloat16)
    )
    packed_heads, values_heads, grad_heads = (
        lax.all_to_all(packed, "sp", split_axis=2, concat_axis=1, tiled=True),
        *side_by_side_2((values, out_grad), "sp", 2, 1, 0),
    )
    heads_here = head_total // sp_count
    lambda_here = lax.dynamic_slice_in_dim(lambdas, lax.axis_index("sp") * heads_here, heads_here)
    seq_length = tok_rows * sp_count
    cosine_all, sine_all = rotation_tables(jnp.arange(seq_length, dtype=jnp.int32), DQK)
    head_split = packed_heads[0].reshape(seq_length, heads_here, 2, 2 * DQK)
    query_heads = head_split[:, :, 0].reshape(seq_length, heads_here * 2 * DQK)
    key_heads = head_split[:, :, 1].reshape(seq_length, heads_here * 2 * DQK)
    query_back, key_back, values_back = head_backward(
        query_heads, key_heads, values_heads[0], grad_heads[0], lambda_here, cosine_all, sine_all
    )
    packed_back = jnp.stack(
        (
            query_back.reshape(seq_length, heads_here, 2 * DQK),
            key_back.reshape(seq_length, heads_here, 2 * DQK),
        ),
        axis=2,
    )
    packed_back = packed_back.reshape(1, seq_length, heads_here * 4 * DQK)
    packed_tokens, values_grad = (
        lax.all_to_all(packed_back, "sp", split_axis=1, concat_axis=2, tiled=True),
        lax.all_to_all(values_back[None], "sp", split_axis=1, concat_axis=2, tiled=True),
    )
    packed_rows = packed_tokens[0]
    back_split = packed_rows.reshape(tok_rows, head_total, 2, 2 * DQK)
    query_tok = back_split[:, :, 0].reshape(tok_rows, head_total * 2 * DQK)
    key_tok = back_split[:, :, 1].reshape(tok_rows, head_total * 2 * DQK)
    contract = (((1,), (1,)), ((), ()))
    tokens_grad = lax.dot_general(
        query_tok, whole_query, contract, preferred_element_type=jnp.float32
    ) + lax.dot_general(key_tok, whole_key, contract, preferred_element_type=jnp.float32)
    outer_rows = (((0,), (0,)), ((), ()))
    grad_shard = lax.psum_scatter(
        lax.dot_general(
            token_block, packed_rows, outer_rows, preferred_element_type=jnp.float32
        ).astype(jnp.bfloat16),
        "dp",
        scatter_dimension=0,
        tiled=True,
    )
    grad_total = lax.psum(grad_shard, "sp").astype(jnp.float32)
    factor = 1.0 / math.sqrt(dp_count * seq_length)
    total_split = grad_total.reshape(grad_total.shape[0], head_total, 2, 2 * DQK)
    query_weight_grad = (
        total_split[:, :, 0].reshape(grad_total.shape[0], head_total * 2 * DQK) * factor
    )
    key_weight_grad = (
        total_split[:, :, 1].reshape(grad_total.shape[0], head_total * 2 * DQK) * factor
    )
    return (tokens_grad.astype(jnp.bfloat16)[None], values_grad, query_weight_grad, key_weight_grad)


def solution(mesh):
    in_specs = (
        P("dp", "sp", None),
        P("dp", None),
        P("dp", None),
        P("dp", "sp", None),
        P(),
        P("dp", "sp", None),
    )
    out_specs = (P("dp", "sp", None), P("dp", "sp", None), P("dp", None), P("dp", None))
    return jax.shard_map(body, mesh=mesh, in_specs=in_specs, out_specs=out_specs, check_vma=False)
```

profile of v0, /device:TPU:1, one launch (start us, length us, event | category | flops | bytes accessed | tf_op | source)
XLA Modules:
  0.0 526.0 jit_solution(12382780276672048796)
XLA Ops:
  12.3 7.6 %all-to-all-start.1 = ((bf16[2,160,1024]{1,0,2:T(2,128)(2,1)}), bf16[2,160,1024]{1,0,2:T(2,128)(2,1)}, u32[]{:S(2)}, u32[]{:S(2)}) async-start(bf16[2,160,1024]{1,0,2:T(2,128)(2,1)} %copy.104), calls=%async_computation.1 | async-start | bytes 2097152 | tf_op jit(solution)/shard_map/all_to_all | solution.py:27
  20.2 50.3 %all-gather.2.cloned.1.call-done = bf16[2048,2048]{1,0:T(8,128)(2,1)} async-done(((bf16[128,2048]{1,0:T(8,128)(2,1)}), bf16[2048,2048]{1,0:T(8,128)(2,1)}) %all-gather.2.cloned.1.call-update) | async-done | bytes 8388624 | tf_op jit(solution)/shard_map/all_gather | solution.py:21
  78.1 11.7 %copy.136 = bf16[1,160,2048]{1,0,2:T(2,128)(2,1)S(1)} copy(bf16[1,160,2048]{1,2,0:T(8,128)(2,1)S(1)} %bitcast.242) | data formatting | bytes 1310720 | tf_op jit(solution)/shard_map/convert_element_type | solution.py:151
  90.4 12.6 %reduce.16 = bf16[2048,160]{1,0:T(8,128)(2,1)} reduce(bf16[2048,1,160]{2,1,0:T(2,128)(2,1)S(1)} %bitcast.233, bf16[]{:T(256)} %broadcast.248), dimensions={1}, to_apply=%bitcast.182.reduce_sub_computation | reduce | bytes 1310722
  103.0 3.9 reshape.418
  106.9 6.6 %all-to-all-start = ((bf16[16,2,10240]{2,1,0:T(2,128)(2,1)}), bf16[16,2,10240]{2,1,0:T(2,128)(2,1)}, u32[]{:S(2)}, u32[]{:S(2)}) async-start(bf16[16,2,10240]{2,1,0:T(2,128)(2,1)} %reshape.418), calls=%async_computation | async-start | bytes 1310720 | tf_op jit(solution)/shard_map/all_to_all | solution.py:154
  126.2 6.0 %reshape.419 = bf16[2048,1,160]{2,1,0:T(2,128)(2,1)} reshape(bf16[16,2,10240]{2,1,0:T(2,128)(2,1)} %all-to-all-done) | data formatting | bytes 1310720
  132.2 4.5 copy.102
  145.4 150.9 %while.16 = (s32[]{:T(128)}, f32[2560,1,2,32]{0,3,2,1:T(8,128)S(1)}, f32[2560,1,64]{0,2,1:T(8,128)}, f32[5,512,1,2,32]{1,0,4,3,2:T(8,128)}, bf16[5,512,1,2,32]{1...) while((s32[]{:T(128)}, ...), condition=%wide.region_7.8_spmd.clone, body=%wide.region_0.7_spmd.clone.sunk | while | flops 1050910720 | bytes 137724240 | solution.py:122
  147.6 9.3 %divide_bitcast_fusion.2 = f32[1,2,512,2560]{3,2,1,0:T(8,128)} fusion(pred[512,2560]{1,0:T(8,128)(4,1)S(1)} %iota_compare_fusion.2, bf16[2560,1,2,32]{0,3,2,1:T(8,128)(2,1)} %get-tuple-element.408, bf16[5,512,1,2,32]{1,4,3,2,0:T(8,128)(2,1)} %get-tuple-element.406, s32[]{:T(128)S(6)} %copy.144), kind=kOutput, calls=%fused_computation.5.clone.1 | convolution fusion | flops 178265088 | bytes 12189700 | tf_op jit(solution)/shard_map/while/body/eval_jaxpr/div | solution.py:89
  156.9 6.6 %fusion.135 = bf16[512,2560]{1,0:T(8,128)(2,1)S(1)} fusion(f32[1,2,512,2560]{3,2,1,0:T(8,128)} %divide_bitcast_fusion.2, f32[]{:T(128)} %bitcast.228), kind=kLoop, calls=%fused_computation.27.clone.1 | loop fusion | flops 3932160 | bytes 13107204 | tf_op jit(solution)/shard_map/while/body/eval_jaxpr/convert_element_type | solution.py:90
  171.9 3.8 dynamic_update_slice.7
  177.7 9.3 %divide_bitcast_fusion.2 = f32[1,2,512,2560]{3,2,1,0:T(8,128)} fusion(pred[512,2560]{1,0:T(8,128)(4,1)S(1)} %iota_compare_fusion.2, bf16[2560,1,2,32]{0,3,2,1:T(8,128)(2,1)} %get-tuple-element.408, bf16[5,512,1,2,32]{1,4,3,2,0:T(8,128)(2,1)} %get-tuple-element.406, s32[]{:T(128)S(6)} %copy.144), kind=kOutput, calls=%fused_computation.5.clone.1 | convolution fusion | flops 178265088 | bytes 12189700 | tf_op jit(solution)/shard_map/while/body/eval_jaxpr/div | solution.py:89
  187.0 6.6 %fusion.135 = bf16[512,2560]{1,0:T(8,128)(2,1)S(1)} fusion(f32[1,2,512,2560]{3,2,1,0:T(8,128)} %divide_bitcast_fusion.2, f32[]{:T(128)} %bitcast.228), kind=kLoop, calls=%fused_computation.27.clone.1 | loop fusion | flops 3932160 | bytes 13107204 | tf_op jit(solution)/shard_map/while/body/eval_jaxpr/convert_element_type | solution.py:90
  207.9 9.3 %divide_bitcast_fusion.2 = f32[1,2,512,2560]{3,2,1,0:T(8,128)} fusion(pred[512,2560]{1,0:T(8,128)(4,1)S(1)} %iota_compare_fusion.2, bf16[2560,1,2,32]{0,3,2,1:T(8,128)(2,1)} %get-tuple-element.408, bf16[5,512,1,2,32]{1,4,3,2,0:T(8,128)(2,1)} %get-tuple-element.406, s32[]{:T(128)S(6)} %copy.144), kind=kOutput, calls=%fused_computation.5.clone.1 | convolution fusion | flops 178265088 | bytes 12189700 | tf_op jit(solution)/shard_map/while/body/eval_jaxpr/div | solution.py:89
  217.2 6.6 %fusion.135 = bf16[512,2560]{1,0:T(8,128)(2,1)S(1)} fusion(f32[1,2,512,2560]{3,2,1,0:T(8,128)} %divide_bitcast_fusion.2, f32[]{:T(128)} %bitcast.228), kind=kLoop, calls=%fused_computation.27.clone.1 | loop fusion | flops 3932160 | bytes 13107204 | tf_op jit(solution)/shard_map/while/body/eval_jaxpr/convert_element_type | solution.py:90
  232.2 3.8 dynamic_update_slice.7
  238.0 9.3 %divide_bitcast_fusion.2 = f32[1,2,512,2560]{3,2,1,0:T(8,128)} fusion(pred[512,2560]{1,0:T(8,128)(4,1)S(1)} %iota_compare_fusion.2, bf16[2560,1,2,32]{0,3,2,1:T(8,128)(2,1)} %get-tuple-element.408, bf16[5,512,1,2,32]{1,4,3,2,0:T(8,128)(2,1)} %get-tuple-element.406, s32[]{:T(128)S(6)} %copy.144), kind=kOutput, calls=%fused_computation.5.clone.1 | convolution fusion | flops 178265088 | bytes 12189700 | tf_op jit(solution)/shard_map/while/body/eval_jaxpr/div | solution.py:89
  247.3 6.6 %fusion.135 = bf16[512,2560]{1,0:T(8,128)(2,1)S(1)} fusion(f32[1,2,512,2560]{3,2,1,0:T(8,128)} %divide_bitcast_fusion.2, f32[]{:T(128)} %bitcast.228), kind=kLoop, calls=%fused_computation.27.clone.1 | loop fusion | flops 3932160 | bytes 13107204 | tf_op jit(solution)/shard_map/while/body/eval_jaxpr/convert_element_type | solution.py:90
  262.3 3.8 dynamic_update_slice.7
  268.1 9.3 %divide_bitcast_fusion.2 = f32[1,2,512,2560]{3,2,1,0:T(8,128)} fusion(pred[512,2560]{1,0:T(8,128)(4,1)S(1)} %iota_compare_fusion.2, bf16[2560,1,2,32]{0,3,2,1:T(8,128)(2,1)} %get-tuple-element.408, bf16[5,512,1,2,32]{1,4,3,2,0:T(8,128)(2,1)} %get-tuple-element.406, s32[]{:T(128)S(6)} %copy.144), kind=kOutput, calls=%fused_computation.5.clone.1 | convolution fusion | flops 178265088 | bytes 12189700 | tf_op jit(solution)/shard_map/while/body/eval_jaxpr/div | solution.py:89
  277.4 6.6 %fusion.135 = bf16[512,2560]{1,0:T(8,128)(2,1)S(1)} fusion(f32[1,2,512,2560]{3,2,1,0:T(8,128)} %divide_bitcast_fusion.2, f32[]{:T(128)} %bitcast.228), kind=kLoop, calls=%fused_computation.27.clone.1 | loop fusion | flops 3932160 | bytes 13107204 | tf_op jit(solution)/shard_map/while/body/eval_jaxpr/convert_element_type | solution.py:90
  292.5 3.8 dynamic_update_slice.7
  300.0 14.5 %reduce.17 = bf16[2560,128]{1,0:T(8,128)(2,1)S(1)} reduce(bf16[2560,1,128]{2,1,0:T(2,128)(2,1)S(1)} %bitcast.239, bf16[]{:T(256)} %broadcast.248), dimensions={1}, to_apply=%bitcast.167.reduce_sub_computation | reduce | bytes 1310722
  314.7 18.1 %all_to_all.63 = bf16[16,2,10240]{2,1,0:T(2,128)(2,1)S(1)} all-to-all(bf16[16,2,10240]{2,1,0:T(2,128)(2,1)S(1)} %reshape.420), channel_id=1, replica_groups=mesh['sp'=16,'dp'=16] {'sp'}, dimensions={0} | all-to-all | bytes 1310720 | tf_op jit(solution)/shard_map/all_to_all | solution.py:176
  333.8 5.6 %convert_bitcast_fusion = bf16[2048,2048]{0,1:T(8,128)(2,1)} fusion(bf16[20,8,16,128]{3,2,1,0:T(8,128)(2,1)S(1)} %bitcast.246, bf16[1,160,2048]{2,1,0:T(8,128)(2,1)S(1)} %copy-done), kind=kOutput, calls=%fused_computation.71 | convolution fusion | flops 1346371584 | bytes 9699328 | tf_op jit(solution)/shard_map/dot_general | solution.py:189
  339.4 12.3 %copy.124 = bf16[2048,2048]{1,0:T(8,128)(2,1)} copy(bf16[2048,2048]{0,1:T(8,128)(2,1)} %convert_bitcast_fusion) | data formatting | bytes 16777216
  356.2 14.3 %reduce.18 = bf16[2560,64]{1,0:T(8,128)(2,1)S(1)} reduce(bf16[2560,1,64]{2,1,0:T(2,128)(2,1)S(1)} %bitcast.238, bf16[]{:T(256)} %broadcast.248), dimensions={1}, to_apply=%bitcast.169.reduce_sub_computation | reduce | bytes 655362
  370.9 10.9 %all_to_all.64 = bf16[16,2,5120]{2,1,0:T(2,128)(2,1)S(1)} all-to-all(bf16[16,2,5120]{2,1,0:T(2,128)(2,1)S(1)} %reshape.422), channel_id=1, replica_groups=mesh['sp'=16,'dp'=16] {'sp'}, dimensions={0} | all-to-all | bytes 655360 | tf_op jit(solution)/shard_map/all_to_all | solution.py:177
  386.6 29.9 %reduce-scatter.4.cloned.1.call-done = bf16[128,2048]{1,0:T(8,128)(2,1)} async-done(((bf16[2048,2048]{1,0:T(8,128)(2,1)}), bf16[128,2048]{1,0:T(8,128)(2,1)}) %reduce-scatter.4.cloned.1.call-update) | async-done | bytes 524304
  422.3 4.6 fusion.85
  426.9 88.9 %all-reduce.2.cloned.1.call-done = bf16[128,16,2,64]{0,3,2,1:T(8,128)(2,1)} async-done(((bf16[128,16,2,64]{0,3,2,1:T(8,128)(2,1)}), bf16[128,16,2,64]{0,3,2,1:T(8,128)(2,1)}) %all-reduce.2.cloned.1.call-update) | async-done | bytes 524304 | tf_op jit(solution)/shard_map/psum | solution.py:196
  (204 shorter events, 113.3 us)
Async XLA Ops:
  7.2 63.3 %copy-start = (bf16[1,160,2048]{2,1,0:T(8,128)(2,1)S(1)}, bf16[1,160,2048]{2,1,0:T(8,128)(2,1)}, u32[]{:S(2)}) copy-start(bf16[1,160,2048]{2,1,0:T(8,128)(2,1)} %param.8) | copy-start | bytes 1966084
  7.2 63.3 %all-gather.2.cloned.1.call-start = ((), (), s32[]{:S(2)}) async-start(), calls=%async_computation.5 | async-start | bytes 8912896 | tf_op jit(solution)/shard_map/all_gather | solution.py:21
  12.3 94.5 %all-to-all-start.1 = ((bf16[2,160,1024]{1,0,2:T(2,128)(2,1)}), bf16[2,160,1024]{1,0,2:T(2,128)(2,1)}, u32[]{:S(2)}, u32[]{:S(2)}) async-start(bf16[2,160,1024]{1,0,2:T(2,128)(2,1)} %copy.104), calls=%async_computation.1 | async-start | bytes 2097152 | tf_op jit(solution)/shard_map/all_to_all | solution.py:27
  78.0 37.3 %copy-start.6 = (f32[16]{0:T(128)S(1)}, f32[16]{0:T(128)}, u32[]{:S(2)}) copy-start(f32[16]{0:T(128)} %param.12) | copy-start | bytes 196
  106.9 19.3 %all-to-all-start = ((bf16[16,2,10240]{2,1,0:T(2,128)(2,1)}), bf16[16,2,10240]{2,1,0:T(2,128)(2,1)}, u32[]{:S(2)}, u32[]{:S(2)}) async-start(bf16[16,2,10240]{2,1,0:T(2,128)(2,1)} %reshape.418), calls=%async_computation | async-start | bytes 1310720 | tf_op jit(solution)/shard_map/all_to_all | solution.py:154
  113.5 303.1 %reduce-scatter.4.cloned.1.call-start = ((), (), s32[]{:S(2)}) async-start(), calls=%async_computation.7 | async-start | bytes 8912896
  145.4 152.4 %copy-start.4 = (f32[2560,16]{0,1:T(8,128)S(1)}, f32[2560,16]{0,1:T(8,128)}, u32[]{:S(2)}) copy-start(f32[2560,16]{0,1:T(8,128)} %get-tuple-element.281) | copy-start | bytes 491524
  156.9 7.6 %copy-start.1 = (f32[2560,1,64]{0,2,1:T(8,128)S(1)}, f32[2560,1,64]{0,2,1:T(8,128)}, u32[]{:S(2)}) copy-start(f32[2560,1,64]{0,2,1:T(8,128)} %get-tuple-element.391) | copy-start | bytes 1966084 | tf_op jit(solution)/shard_map/while
  156.9 8.2 %slice-start = ((s8[10485760]{0:T(1024)(128)(4,1)}), s8[4194304]{0:T(1024)(128)(4,1)S(1)}, s32[]{:S(2)}) async-start(s8[10485760]{0:T(1024)(128)(4,1)} %bitcast.230), calls=%async_computation.8 | async-start | bytes 8388608 | tf_op jit(solution)/shard_map/while
  156.9 8.2 %slice-start.1 = ((s8[10485760]{0:T(1024)(128)(4,1)}), s8[2097152]{0:T(1024)(128)(4,1)S(1)}, s32[]{:S(2)}) async-start(s8[10485760]{0:T(1024)(128)(4,1)} %bitcast.230), calls=%async_computation.9 | async-start | bytes 4194304 | tf_op jit(solution)/shard_map/while
  163.5 2.2 slice-start.2
  166.7 1.3 copy-start.5
  187.0 7.6 %copy-start.1 = (f32[2560,1,64]{0,2,1:T(8,128)S(1)}, f32[2560,1,64]{0,2,1:T(8,128)}, u32[]{:S(2)}) copy-start(f32[2560,1,64]{0,2,1:T(8,128)} %get-tuple-element.391) | copy-start | bytes 1966084 | tf_op jit(solution)/shard_map/while
  187.0 8.2 %slice-start = ((s8[10485760]{0:T(1024)(128)(4,1)}), s8[4194304]{0:T(1024)(128)(4,1)S(1)}, s32[]{:S(2)}) async-start(s8[10485760]{0:T(1024)(128)(4,1)} %bitcast.230), calls=%async_computation.8 | async-start | bytes 8388608 | tf_op jit(solution)/shard_map/while
  187.0 8.2 %slice-start.1 = ((s8[10485760]{0:T(1024)(128)(4,1)}), s8[2097152]{0:T(1024)(128)(4,1)S(1)}, s32[]{:S(2)}) async-start(s8[10485760]{0:T(1024)(128)(4,1)} %bitcast.230), calls=%async_computation.9 | async-start | bytes 4194304 | tf_op jit(solution)/shard_map/while
  193.6 2.2 slice-start.2
  196.9 1.3 copy-start.5
  217.2 7.6 %copy-start.1 = (f32[2560,1,64]{0,2,1:T(8,128)S(1)}, f32[2560,1,64]{0,2,1:T(8,128)}, u32[]{:S(2)}) copy-start(f32[2560,1,64]{0,2,1:T(8,128)} %get-tuple-element.391) | copy-start | bytes 1966084 | tf_op jit(solution)/shard_map/while
  217.2 8.2 %slice-start = ((s8[10485760]{0:T(1024)(128)(4,1)}), s8[4194304]{0:T(1024)(128)(4,1)S(1)}, s32[]{:S(2)}) async-start(s8[10485760]{0:T(1024)(128)(4,1)} %bitcast.230), calls=%async_computation.8 | async-start | bytes 8388608 | tf_op jit(solution)/shard_map/while
  217.2 8.2 %slice-start.1 = ((s8[10485760]{0:T(1024)(128)(4,1)}), s8[2097152]{0:T(1024)(128)(4,1)S(1)}, s32[]{:S(2)}) async-start(s8[10485760]{0:T(1024)(128)(4,1)} %bitcast.230), calls=%async_computation.9 | async-start | bytes 4194304 | tf_op jit(solution)/shard_map/while
  223.7 2.2 slice-start.2
  227.0 1.3 copy-start.5
  247.3 7.6 %copy-start.1 = (f32[2560,1,64]{0,2,1:T(8,128)S(1)}, f32[2560,1,64]{0,2,1:T(8,128)}, u32[]{:S(2)}) copy-start(f32[2560,1,64]{0,2,1:T(8,128)} %get-tuple-element.391) | copy-start | bytes 1966084 | tf_op jit(solution)/shard_map/while
  247.3 8.2 %slice-start = ((s8[10485760]{0:T(1024)(128)(4,1)}), s8[4194304]{0:T(1024)(128)(4,1)S(1)}, s32[]{:S(2)}) async-start(s8[10485760]{0:T(1024)(128)(4,1)} %bitcast.230), calls=%async_computation.8 | async-start | bytes 8388608 | tf_op jit(solution)/shard_map/while
  247.3 8.2 %slice-start.1 = ((s8[10485760]{0:T(1024)(128)(4,1)}), s8[2097152]{0:T(1024)(128)(4,1)S(1)}, s32[]{:S(2)}) async-start(s8[10485760]{0:T(1024)(128)(4,1)} %bitcast.230), calls=%async_computation.9 | async-start | bytes 4194304 | tf_op jit(solution)/shard_map/while
  253.9 2.2 slice-start.2
  257.1 1.3 copy-start.5
  277.4 7.6 %copy-start.1 = (f32[2560,1,64]{0,2,1:T(8,128)S(1)}, f32[2560,1,64]{0,2,1:T(8,128)}, u32[]{:S(2)}) copy-start(f32[2560,1,64]{0,2,1:T(8,128)} %get-tuple-element.391) | copy-start | bytes 1966084 | tf_op jit(solution)/shard_map/while
  277.4 8.2 %slice-start = ((s8[10485760]{0:T(1024)(128)(4,1)}), s8[4194304]{0:T(1024)(128)(4,1)S(1)}, s32[]{:S(2)}) async-start(s8[10485760]{0:T(1024)(128)(4,1)} %bitcast.230), calls=%async_computation.8 | async-start | bytes 8388608 | tf_op jit(solution)/shard_map/while
  277.4 8.2 %slice-start.1 = ((s8[10485760]{0:T(1024)(128)(4,1)}), s8[2097152]{0:T(1024)(128)(4,1)S(1)}, s32[]{:S(2)}) async-start(s8[10485760]{0:T(1024)(128)(4,1)} %bitcast.230), calls=%async_computation.9 | async-start | bytes 4194304 | tf_op jit(solution)/shard_map/while
  284.0 2.2 slice-start.2
  351.7 164.1 %all-reduce.2.cloned.1.call-start = ((), (), s32[]{:S(2)}) async-start(), calls=%async_computation.6 | async-start | bytes 1048576 | tf_op jit(solution)/shard_map/psum | solution.py:196
  (7 other events, 7.7 us)
Sparse Core Ops, SparseCore 0:
  10.4 60.0 all-gather.1
  351.8 64.6 reduce-scatter.3
  420.3 95.4 all-reduce.1
where the time goes:
time: 536 us; the launch traced here: 526 us
  waiting for transfers between devices  169 us (32%)
  local copies, waits for them, and re-layouts  102 us (19%)
  matrix products  98.5 us (18%)
  other arithmetic  96.1 us (18%)
  blocking collectives  29 us (5%)
  between operations  15.3 us (3%)
  starting transfers between devices  14.8 us (3%)
    psum x1, waiting for transfers between devices, body(): grad_total = lax.psum(grad_shard, 'sp').astype(jnp.float32)  88.9 us
    all_gather x1, waiting for transfers between devices, side_by_side(): lax.all_gather(both, axis, axis=dim, tiled=True)  50.3 us
    div x5, matrix products, block_step(): prob_maps = exp_scores / jnp.sum(exp_scores, axis=-1, keepdims=True)  46.6 us
    unnamed x5, other arithmetic  41.4 us
    convert_element_type x5, other arithmetic, block_step(): (prob_maps[:, 0] - lambda_col * prob_maps[:, 1]).astype(jnp.bfloat16)  32.8 us
    dot_general x25, matrix products, pair_product(): jnp.einsum(pattern, first_op, second_op, preferred_element_type=jnp.float32)  32 us
    unnamed x23, local copies, waits for them, and re-layouts  30.8 us
    unnamed x4, waiting for transfers between devices  30 us
  transfers between devices with their start and end apart: 5, of which 3 were waited for; matrix products, arithmetic and copies ran while one was open for 15% of the time, Pallas kernels for 0%

commit v1 on v0

v1 whole, which is shorter than its diff:
```python
import math

import jax
import jax.numpy as jnp
from jax import lax
from jax.experimental import pallas as pl
from jax.experimental.pallas import tpu as pltpu
from jax.sharding import PartitionSpec as P

THETA = 10000.0
DQK = 32
NORM_EPS = 0.1
F32, BF16 = jnp.float32, jnp.bfloat16
SEQ = 2560
BQ = 256
BK = 512
NB = SEQ // BQ


def mm(a, b, dims=(((1,), (0,)), ((), ()))):
    return lax.dot_general(a, b, dims, preferred_element_type=F32)


def rot_t(x, c, s, sign):
    parts = []
    for base in range(0, x.shape[0], 32):
        a, b = x[base:base + 16], x[base + 16:base + 32]
        parts += [a * c - b * (sign * s), b * c + a * (sign * s)]
    return jnp.concatenate(parts, axis=0)


def fold(x, op):
    r = x.reshape(x.shape[0] // 8, 8, x.shape[1])
    return op(r, axis=0)


def attention(lam, rot_ref, rotT_ref, vg_ref, vgT_ref, cosT, sinT, dqT_ref, acc_ref, e1_ref, e2_ref, mix_ref, dp_ref):
    inv_root = 1.0 / math.sqrt(32)
    c2 = inv_root * math.log2(math.e)
    acc_ref[...] = jnp.zeros_like(acc_ref)
    zq = jnp.zeros((32, BQ), BF16)

    def block(step, _):
        b = NB - 1 - step
        qs = pl.multiple_of(b * BQ, BQ)
        qcols = pl.ds(qs, BQ)
        last = b // 2
        q1T = rotT_ref[0:32, qcols]
        q2T = rotT_ref[32:64, qcols]
        rhs1 = jnp.concatenate([zq, zq, q1T, zq], axis=0)
        rhs2 = jnp.concatenate([zq, zq, zq, q2T], axis=0)

        def scores(j):
            ks = pl.multiple_of(j * BK, BK)
            kk = rot_ref[pl.ds(ks, BK), :]
            return ks, mm(kk, rhs1), mm(kk, rhs2)

        def ph1(j, c):
            m1, m2 = c
            ks, s1, s2 = scores(j)
            e1_ref[pl.ds(ks, BK), :] = s1
            e2_ref[pl.ds(ks, BK), :] = s2
            return jnp.maximum(m1, fold(s1, jnp.max)), jnp.maximum(m2, fold(s2, jnp.max))

        neg = jnp.full((8, BQ), -jnp.inf, F32)
        m1, m2 = lax.fori_loop(0, last, ph1, (neg, neg))
        ks, s1, s2 = scores(last)
        mask = (ks + lax.broadcasted_iota(jnp.int32, (BK, BQ), 0)) <= (qs + lax.broadcasted_iota(jnp.int32, (BK, BQ), 1))
        s1 = jnp.where(mask, s1, -jnp.inf)
        s2 = jnp.where(mask, s2, -jnp.inf)
        e1_ref[pl.ds(ks, BK), :] = s1
        e2_ref[pl.ds(ks, BK), :] = s2
        m1 = jnp.max(jnp.maximum(m1, fold(s1, jnp.max)), axis=0, keepdims=True)
        m2 = jnp.max(jnp.maximum(m2, fold(s2, jnp.max)), axis=0, keepdims=True)

        def ph2(j, c):
            l1, l2 = c
            rows = pl.ds(pl.multiple_of(j * BK, BK), BK)
            e1 = jnp.exp2((e1_ref[rows, :] - m1) * c2)
            e2 = jnp.exp2((e2_ref[rows, :] - m2) * c2)
            e1_ref[rows, :] = e1
            e2_ref[rows, :] = e2
            return l1 + fold(e1, jnp.sum), l2 + fold(e2, jnp.sum)

        zero = jnp.zeros((8, BQ), F32)
        l1, l2 = lax.fori_loop(0, last + 1, ph2, (zero, zero))
        r1 = 1.0 / jnp.sum(l1, axis=0, keepdims=True)
        r2 = lam / jnp.sum(l2, axis=0, keepdims=True)

        def ph3(j, o):
            rows = pl.ds(pl.multiple_of(j * BK, BK), BK)
            mix = (e1_ref[rows, :] * r1 - e2_ref[rows, :] * r2).astype(BF16)
            mix_ref[rows, :] = mix
            return o + mm(vgT_ref[0:64, rows], mix)

        o = lax.fori_loop(0, last + 1, ph3, jnp.zeros((64, BQ), F32))
        g = vgT_ref[64:128, qcols].astype(F32)
        ns = lax.rsqrt(jnp.mean(o * o, axis=0, keepdims=True) + NORM_EPS)
        ob = ns * g - ns * ns * ns * o * jnp.mean(g * o, axis=0, keepdims=True)
        obT = ob.astype(BF16)
        obp = jnp.concatenate([jnp.zeros((64, BQ), F32), ob], axis=0).T.astype(BF16)
        obz = jnp.concatenate([obT, jnp.zeros((64, BQ), BF16)], axis=0)

        def ph4(j, c):
            d1, d2 = c
            rows = pl.ds(pl.multiple_of(j * BK, BK), BK)
            dp = mm(vg_ref[rows, :], obz)
            dp_ref[rows, :] = dp
            return d1 + fold(dp * e1_ref[rows, :], jnp.sum), d2 + fold(dp * e2_ref[rows, :], jnp.sum)

        d1, d2 = lax.fori_loop(0, last + 1, ph4, (zero, zero))
        r2n = -r2
        d1 = jnp.sum(d1, axis=0, keepdims=True) * r1
        d2 = jnp.sum(d2, axis=0, keepdims=True) * (1.0 / jnp.sum(l2, axis=0, keepdims=True))
        f1 = r1 * inv_root
        f2 = r2n * inv_root
        lane = lax.broadcasted_iota(jnp.int32, (BQ, 128), 1)
        qrows = rot_ref[qcols, :]
        zb = jnp.zeros_like(qrows)
        rhs = jnp.concatenate([jnp.where(lane < 32, qrows, zb), jnp.where((lane >= 32) & (lane < 64), qrows, zb), obp], axis=0)

        def ph5(j, c):
            a1, a2 = c
            rows = pl.ds(pl.multiple_of(j * BK, BK), BK)
            dp = dp_ref[rows, :]
            g1 = (e1_ref[rows, :] * f1 * (dp - d1)).astype(BF16)
            g2 = (e2_ref[rows, :] * f2 * (dp - d2)).astype(BF16)
            lhs = jnp.concatenate([g1, g2, mix_ref[rows, :]], axis=1)
            acc_ref[rows, :] += mm(lhs, rhs)
            return a1 + mm(rotT_ref[64:96, rows], g1), a2 + mm(rotT_ref[96:128, rows], g2)

        za = jnp.zeros((32, BQ), F32)
        a1, a2 = lax.fori_loop(0, last + 1, ph5, (za, za))
        dqT_ref[0:32, qcols] = a1
        dqT_ref[32:64, qcols] = a2
        return 0

    lax.fori_loop(0, NB, block, 0)


TOK = 160
HALF = 80
D = 2048
COLS = 1024
TRANS_B = (((1,), (1,)), ((), ()))


def spot(q, c):
    q = lax.rem(q + 32, 16)
    u = lax.div(q, 4)
    w = lax.rem(lax.rem(q, 4) - u + 4, 4)
    y = u * (1 - c) + w * c
    x = w * (1 - c) + u * c
    return 4 * y + x


def join(a, b):
    return jnp.concatenate([a[:, :64], b[:, :64]], axis=1), jnp.concatenate([a[:, 64:], b[:, 64:]], axis=1)


def kernel(factor, lam_ref, tok_ref, wq_ref, wk_ref, v_ref, g_ref, cosT, sinT,
           tg_ref, vgrad_ref, dwq_ref, dwk_ref,
           tokF, wqF, wkF, whead, xf, vgpack, vgF, rot, rotT, vgT, dqT, acc, e1, e2, mix, dp,
           backT, bpack, bF, dwp, dwR, dwS, dwG,
           tsend, trecv, wsend, wrecv, psend, precv, asend, arecv, bsend, brecv, rsend, rrecv, gsend, grecv, lsem):
    sp = lax.axis_index("sp")
    dpi = lax.axis_index("dp")
    core = lax.rem(dpi, 2)
    z = lax.div(dpi, 2)
    mate = z * 2 + 1 - core
    y, x = lax.div(sp, 4), lax.rem(sp, 4)
    u = y * (1 - core) + x * core
    w = x * (1 - core) + y * core
    place = 4 * u + lax.rem(u + w, 4)

    barrier = pltpu.get_barrier_semaphore()
    for d in range(1, 16):
        pl.semaphore_signal(barrier, inc=1, device_id={"sp": lax.rem(sp + d, 16)}, device_id_type=pl.DeviceIdType.MESH)
        pl.semaphore_signal(barrier, inc=1, device_id={"dp": lax.rem(dpi + d, 16)}, device_id_type=pl.DeviceIdType.MESH)
    pl.semaphore_wait(barrier, 30)

    sends = []

    def send(src, dst, ss, rs, to):
        c = pltpu.make_async_remote_copy(src_ref=src, dst_ref=dst, send_sem=ss, recv_sem=rs, device_id=to,
                                         device_id_type=pl.DeviceIdType.MESH)
        c.start()
        sends.append(c)

    def arrive(dst, ss, rs):
        pltpu.make_async_remote_copy(src_ref=dst, dst_ref=dst, send_sem=ss, recv_sem=rs, device_id={"sp": sp},
                                     device_id_type=pl.DeviceIdType.MESH).wait_recv()

    nxt = ({"sp": spot(place + 1, core)}, {"sp": spot(place - 1, core)})

    def tok_part(back, d, half):
        origin = spot(place - back, core) if d == 0 else spot(place + back, core)
        return pl.ds(pl.multiple_of(origin * TOK + half * HALF, HALF), HALF)

    def tok_half(d, k):
        return d if k == 14 else k % 2

    def tok_send(d, k):
        half = tok_half(d, k)
        rows = tok_part(k // 2, d, half)
        src = tok_ref.at[pl.ds(half * HALF, HALF)] if k < 2 else tokF.at[rows]
        send(src, tokF.at[rows], tsend.at[d, k], trecv.at[d, k], nxt[d])

    def tok_wait(d, k):
        rows = tok_part(k // 2 + 1, d, tok_half(d, k))
        arrive(tokF.at[rows], tsend.at[d, k], trecv.at[d, k])

    znext = ({"dp": lax.rem(z + 1, 8) * 2 + core}, {"dp": lax.rem(z + 7, 8) * 2 + core})
    wF = (wqF, wkF)
    wown = (wq_ref, wk_ref)

    def w_rows(owner):
        return pl.ds(pl.multiple_of(owner * 128, 128), 128)

    def w_owner(back, d):
        return lax.rem(z + 8 - back, 8) * 2 + core if d == 0 else lax.rem(z + back, 8) * 2 + core

    def w_which(d, k):
        return d if k == 6 else k % 2

    def w_send(d, k):
        m = w_which(d, k)
        rows = w_rows(w_owner(k // 2, d))
        send(wown[m] if k < 2 else wF[m].at[rows], wF[m].at[rows], wsend.at[d, k], wrecv.at[d, k], znext[d])

    def w_wait(d, k):
        arrive(wF[w_which(d, k)].at[w_rows(w_owner(k // 2 + 1, d))], wsend.at[d, k], wrecv.at[d, k])

    def mate_send(d, k):
        if k < 0:
            m, owner, i = d, dpi, 14 + d
        else:
            m, owner, i = w_which(d, k), w_owner(k // 2 + 1, d), d * 7 + k
        rows = w_rows(owner)
        send(wown[m] if k < 0 else wF[m].at[rows], wF[m].at[rows], psend.at[i], precv.at[i], {"dp": mate})

    def mate_wait(d, k):
        if k < 0:
            m, owner, i = d, mate, 14 + d
        else:
            m, owner, i = w_which(d, k), w_owner(k // 2 + 1, d) + 1 - 2 * core, d * 7 + k
        arrive(wF[m].at[w_rows(owner)], psend.at[i], precv.at[i])

    for k in range(2):
        for d in range(2):
            tok_send(d, k)
            w_send(d, k)
    for m in range(2):
        mate_send(m, -1)
    own = [pltpu.make_async_copy(tok_ref, tokF.at[pl.ds(pl.multiple_of(sp * TOK, TOK), TOK)], lsem.at[0]),
           pltpu.make_async_copy(wq_ref, wqF.at[w_rows(dpi)], lsem.at[1]),
           pltpu.make_async_copy(wk_ref, wkF.at[w_rows(dpi)], lsem.at[2])]
    for c in own:
        c.start()

    for p in range(8):
        lanes = slice(p * 128, (p + 1) * 128)
        vp, gp = v_ref[:, lanes], g_ref[:, lanes]
        vgpack[2 * p], vgpack[2 * p + 1] = join(vp, gp)
    vgF[pl.ds(pl.multiple_of(sp * TOK, TOK), TOK), :] = vgpack[sp]
    for c in own:
        c.wait()

    def peer_rows(i, n):
        return pl.ds(pl.multiple_of(i * n, n), n)

    def vg_send():
        for d in range(1, 16):
            to = lax.rem(sp + d, 16)
            send(vgpack.at[to], vgF.at[peer_rows(sp, TOK)], asend.at[d], arecv.at[d], {"sp": to})

    def vg_wait():
        for d in range(1, 16):
            arrive(vgF.at[peer_rows(lax.rem(sp + 16 - d, 16), TOK)], asend.at[d], arecv.at[d])

        def turn(i, _):
            r = pl.multiple_of(i * 256, 256)
            vgT[:, pl.ds(r, 256)] = vgF[pl.ds(r, 256), :].astype(F32).T.astype(BF16)
            return 0
        lax.fori_loop(0, SEQ // 256, turn, 0)

    def make_head():
        pair = pl.ds(pl.multiple_of(lax.div(sp, 2) * 128, 128), 128)
        odd = lax.rem(sp, 2)

        def part(i, _):
            rows = pl.ds(pl.multiple_of(i * 256, 256), 256)
            lo, hi = join(wqF[rows, pair], wkF[rows, pair])
            whead[rows, :] = jnp.where(odd == 0, lo, hi)
            return 0
        lax.fori_loop(0, 8, part, 0)

    def project(origin):
        rows = pl.ds(pl.multiple_of(origin * TOK, TOK), TOK)
        xf[rows, :] = mm(tokF[rows, :], whead[...])

    ready = [sp]
    after = {0: 0, 2: 1, 3: 2, 5: 3, 7: 4, 8: 5, 10: 6}
    for k in range(15):
        for d in range(2):
            tok_wait(d, k)
            if k + 2 < 14:
                tok_send(d, k + 2)
            elif k + 2 == 14:
                if d == 0:
                    tok_send(d, k + 2)
            elif k == 13:
                if d == 1:
                    tok_send(1, 14)
            if k % 2 == 1:
                ready.append(spot(place - (k // 2 + 1), core) if d == 0 else spot(place + (k // 2 + 1), core))
        if k in after:
            j = after[k]
            for d in range(2):
                w_wait(d, j)
                if j + 2 < 6:
                    w_send(d, j + 2)
                elif j == 4 and d == 0:
                    w_send(0, 6)
                elif j == 5 and d == 1:
                    w_send(1, 6)
                mate_send(d, j)
        if k == 0:
            vg_send()
        if k == 8:
            vg_wait()
        if k == 10:
            for m in range(2):
                mate_wait(m, -1)
            for j in range(7):
                for d in range(2):
                    mate_wait(d, j)
            make_head()
        if k > 10:
            for _ in range(min(4, len(ready))):
                project(ready.pop(0))
    ready.append(spot(place - 8, core))
    for origin in ready:
        project(origin)

    def turn_all(i, _):
        cols = pl.ds(pl.multiple_of(i * 256, 256), 256)
        xt = rot_t(xf[cols, :].T, cosT[:, cols], sinT[:, cols], 1.0)
        rotT[:, cols] = xt.astype(BF16)
        rot[cols, :] = xt.T.astype(BF16)
        return 0
    lax.fori_loop(0, SEQ // 256, turn_all, 0)

    attention(lam_ref[sp], rot, rotT, vgF, vgT, cosT, sinT, dqT, acc, e1, e2, mix, dp)

    def fin(i, _):
        cols = pl.ds(pl.multiple_of(i * 256, 256), 256)
        kvT = acc[cols, :].T
        c, s = cosT[:, cols], sinT[:, cols]
        bt = jnp.concatenate([rot_t(dqT[:, cols], c, s, -1.0), rot_t(kvT[0:64], c, s, -1.0)], axis=0)
        backT[:, cols] = bt.astype(BF16)
        xf[cols, :] = bt.T
        return 0
    lax.fori_loop(0, SEQ // 256, fin, 0)

    def pack(i, _):
        r = pl.multiple_of(i * TOK, TOK)
        bpack[i, 0:TOK, :] = xf[pl.ds(r, TOK), :].astype(BF16)
        dv0 = acc[pl.ds(r, HALF), :]
        dv1 = acc[pl.ds(r + HALF, HALF), :]
        bpack[i, TOK:TOK + HALF, :] = jnp.concatenate([dv0[:, 64:], dv1[:, 64:]], axis=1).astype(BF16)
        return 0
    lax.fori_loop(0, 16, pack, 0)
    bF[sp] = bpack[sp]

    def dw(i, _):
        cols = pl.ds(pl.multiple_of(i * 256, 256), 256)
        r = mm(backT[...], tokF[:, cols]).astype(BF16)
        dwp[2 * i] = r[:, :128]
        dwp[2 * i + 1] = r[:, 128:]
        return 0
    lax.fori_loop(0, 8, dw, 0)

    for d in range(1, 16):
        to = lax.rem(sp + d, 16)
        send(bpack.at[to], bF.at[sp], bsend.at[d], brecv.at[d], {"sp": to})
    for d in range(1, 16):
        to = lax.rem(dpi + d, 16)
        send(dwp.at[to], dwR.at[dpi], rsend.at[d], rrecv.at[d], {"dp": to})
    dwR[dpi] = dwp[dpi]

    for d in range(1, 16):
        arrive(dwR.at[lax.rem(dpi + 16 - d, 16)], rsend.at[d], rrecv.at[d])
    total = dwR[0].astype(F32)
    for i in range(1, 16):
        total += dwR[i].astype(F32)
    dwS[...] = total.T.astype(BF16)
    dwG[sp] = total.T.astype(BF16)
    for d in range(1, 16):
        arrive(bF.at[lax.rem(sp + 16 - d, 16)], bsend.at[d], brecv.at[d])
    for d in range(1, 16):
        send(dwS, dwG.at[sp], gsend.at[d], grecv.at[d], {"sp": lax.rem(sp + d, 16)})

    bq, bk = [], []
    for p in range(8):
        lanes = slice(p * 128, (p + 1) * 128)
        a, b = bF[2 * p], bF[2 * p + 1]
        q, k = join(a[:TOK], b[:TOK])
        bq.append(q)
        bk.append(k)
        top, low = join(a[TOK:], b[TOK:])
        vgrad_ref[0:HALF, lanes] = top
        vgrad_ref[HALF:TOK, lanes] = low
    bq = jnp.concatenate(bq, axis=1)
    bk = jnp.concatenate(bk, axis=1)
    for n in range(8):
        rows = slice(n * 256, (n + 1) * 256)
        tg_ref[:, rows] = (mm(bq, wqF[rows, :], TRANS_B) + mm(bk, wkF[rows, :], TRANS_B)).astype(BF16)

    for d in range(1, 16):
        arrive(dwG.at[lax.rem(sp + 16 - d, 16)], gsend.at[d], grecv.at[d])
    for p in range(8):
        lanes = slice(p * 128, (p + 1) * 128)
        q, k = join(dwG[2 * p].astype(F32), dwG[2 * p + 1].astype(F32))
        dwq_ref[:, lanes] = q * factor
        dwk_ref[:, lanes] = k * factor
    for c in sends:
        c.wait_send()


def body(tokens, query_weight, key_weight, values, lambdas, out_grad):
    half = DQK // 2
    freqs = jnp.exp(-math.log(THETA) * jnp.arange(half, dtype=F32) / half)
    angles = freqs[:, None] * jnp.arange(SEQ, dtype=jnp.int32).astype(F32)[None, :]
    vm = pl.BlockSpec(memory_space=pltpu.VMEM)
    dma = pltpu.SemaphoreType.DMA
    V = pltpu.VMEM
    return_shapes = (
        jax.ShapeDtypeStruct((TOK, D), BF16),
        jax.ShapeDtypeStruct((TOK, COLS), BF16),
        jax.ShapeDtypeStruct((128, COLS), F32),
        jax.ShapeDtypeStruct((128, COLS), F32),
    )
    import functools
    tg, vg, dq, dk = pl.pallas_call(
        functools.partial(kernel, 1.0 / math.sqrt(16 * SEQ)),
        out_shape=return_shapes,
        in_specs=[pl.BlockSpec(memory_space=pltpu.SMEM)] + [vm] * 7,
        out_specs=(vm,) * 4,
        scratch_shapes=[
            V((SEQ, D), BF16), V((D, COLS), BF16), V((D, COLS), BF16), V((D, 128), BF16), V((SEQ, 128), F32),
            V((16, TOK, 128), BF16), V((SEQ, 128), BF16),
            V((SEQ, 128), BF16), V((128, SEQ), BF16), V((128, SEQ), BF16), V((64, SEQ), F32), V((SEQ, 128), F32),
            V((SEQ, BQ), F32), V((SEQ, BQ), F32), V((SEQ, BQ), BF16), V((SEQ, BQ), F32),
            V((128, SEQ), BF16), V((16, TOK + HALF, 128), BF16), V((16, TOK + HALF, 128), BF16),
            V((16, 128, 128), BF16), V((16, 128, 128), BF16), V((128, 128), BF16), V((16, 128, 128), BF16),
            dma((2, 15)), dma((2, 15)), dma((2, 7)), dma((2, 7)), dma((16,)), dma((16,)), dma((16,)), dma((16,)),
            dma((16,)), dma((16,)), dma((16,)), dma((16,)), dma((16,)), dma((16,)), dma((3,)),
        ],
        compiler_params=pltpu.CompilerParams(vmem_limit_bytes=60 * 1024 * 1024, collective_id=0, has_side_effects=True),
        name="differential_backward",
    )(lambdas, tokens[0], query_weight, key_weight, values[0], out_grad[0], jnp.cos(angles), jnp.sin(angles))
    return tg[None], vg[None], dq, dk


def solution(mesh):
    in_specs = (
        P("dp", "sp", None),
        P("dp", None),
        P("dp", None),
        P("dp", "sp", None),
        P(),
        P("dp", "sp", None),
    )
    out_specs = (P("dp", "sp", None), P("dp", "sp", None), P("dp", None), P("dp", None))
    return jax.shard_map(body, mesh=mesh, in_specs=in_specs, out_specs=out_specs, check_vma=False)
```

time: 536 us -> 159 us (0.30); the launches traced: 526 us -> 159 us
  waiting for transfers between devices: 169 us -> 0 us
  Pallas kernels: 0 us -> 151 us
  matrix products: 98.5 us -> 0 us
  local copies, waits for them, and re-layouts: 102 us -> 5.21 us
  other arithmetic: 96.1 us -> 1.39 us
  blocking collectives: 29 us -> 0 us
  starting transfers between devices: 14.8 us -> 0 us
  between operations: 15.3 us -> 0.66 us
    pallas_call x0 -> x1, Pallas kernels: none -> 151 us  [body(): pl.pallas_call(functools.partial(kernel, 1.0 / math.sqrt(16 * SEQ)), out_...]
    psum x1 -> x0, waiting for transfers between devices: 88.9 us -> none  [body(): grad_total = lax.psum(grad_shard, 'sp').astype(jnp.float32)]
    dot_general x30 -> x0, matrix products: 52 us -> none  [the longest x25 32 us: pair_product(): jnp.einsum(pattern, first_op, second_op, preferred_element_type=jnp.float32)]
    all_gather x1 -> x0, waiting for transfers between devices: 50.3 us -> none  [side_by_side(): lax.all_gather(both, axis, axis=dim, tiled=True)]
    div x5 -> x0, matrix products: 46.6 us -> none  [block_step(): prob_maps = exp_scores / jnp.sum(exp_scores, axis=-1, keepdims=True)]
    unnamed x5 -> x0, other arithmetic: 41.4 us -> none
    convert_element_type x8 -> x1, other arithmetic: 33.5 us -> 0.01 us  [body(): jnp.arange(SEQ, dtype=jnp.int32).astype(F32)[None, :]]
    unnamed x4 -> x0, waiting for transfers between devices: 30 us -> none
  transfers between devices with their start and end apart: 5 -> 0, of which waited for: 3 -> 0; matrix products, arithmetic and copies ran while one was open for 15% -> 0% of each run, Pallas kernels for 0% -> 0%
where the time goes in v1:
time: 159 us
  Pallas kernels  151 us (95%)
  local copies, waits for them, and re-layouts  5.21 us (3%)
    pallas_call x1, Pallas kernels, body(): pl.pallas_call(functools.partial(kernel, 1.0 / math.sqrt(16 * SEQ)), out_...  151 us
    unnamed x10, local copies, waits for them, and re-layouts  5.21 us

profile of v1, /device:TPU:1, one launch (start us, length us, event | category | flops | bytes accessed | tf_op | source)
XLA Modules:
  0.0 158.6 jit_solution(512182865941619819)
XLA Ops:
  0.7 1.4 multiply_sine_fusion
  2.0 151.4 %differential_backward.1 = (bf16[160,2048]{1,0:T(8,128)(2,1)}, bf16[160,1024]{1,0:T(8,128)(2,1)}, f32[128,1024]{1,0:T(8,128)}, f32[128,1024]{1,0:T(8,128)}) custom-call(f32[16]{0:T(128)} %lam_ref.1, bf16[160,2048]{1,0:T(8,128)(2,1)} %bitcast.5, bf16[128,1024]{1,0:T(8,128)(2,1)} %wq_ref.1, bf16[128,1024]{1,0:T(8,128)(2,1)} %wk_ref.1, ...), custom_call_target="tpu_custom_call" | custom-call | tf_op jit(solution)/shard_map/differential_backward/pallas_call | solution.py:445
  153.4 0.0 copy-start.2
  153.4 2.0 %copy.14 = bf16[1,160,2048]{2,1,0:T(8,128)(2,1)} copy(bf16[1,160,2048]{2,1,0:T(8,128)(2,1)} %bitcast.6) | data formatting | bytes 1310720
  155.4 0.0 copy-done.2
  155.4 0.0 copy-start.1
  155.4 0.7 copy.15
  156.2 0.4 copy-done.1
  156.6 0.0 copy-start
  156.6 0.8 copy.16
  157.4 0.4 copy-done
  157.8 0.8 copy.17
  (2 shorter events, 0.0 us)
Async XLA Ops:
  153.4 2.0 %copy-start.2 = (bf16[160,1024]{1,0:T(8,128)(2,1)S(1)}, bf16[160,1024]{1,0:T(8,128)(2,1)}, u32[]{:S(2)}) copy-start(bf16[160,1024]{1,0:T(8,128)(2,1)} %get-tuple-element.9) | copy-start | bytes 983044
  155.4 1.2 copy-start.1
  156.6 1.2 copy-start

commit v2 on v1

v2 whole, which is shorter than its diff:
```python
import functools
import math

import jax
import jax.numpy as jnp
from jax import lax
from jax.experimental import pallas as pl
from jax.experimental.pallas import tpu as pltpu
from jax.sharding import PartitionSpec as P

THETA = 10000.0
DQK = 32
NORM_EPS = 0.1
F32, BF16 = jnp.float32, jnp.bfloat16
SEQ = 2560
BQ = 256
BK = 512
NB = SEQ // BQ


def mm(a, b, dims=(((1,), (0,)), ((), ()))):
    return lax.dot_general(a, b, dims, preferred_element_type=F32)


def rot_t(x, c, s, sign):
    parts = []
    for base in range(0, x.shape[0], 32):
        a, b = x[base:base + 16], x[base + 16:base + 32]
        parts += [a * c - b * (sign * s), b * c + a * (sign * s)]
    return jnp.concatenate(parts, axis=0)


def fold(x, op):
    r = x.reshape(x.shape[0] // 8, 8, x.shape[1])
    return op(r, axis=0)


def attention(lam, rot_ref, rotT_ref, vg_ref, vgT_ref, cosT, sinT, dqT_ref, acc_ref, e1_ref, e2_ref, mix_ref, dp_ref, hook):
    inv_root = 1.0 / math.sqrt(32)
    c2 = inv_root * math.log2(math.e)
    acc_ref[...] = jnp.zeros_like(acc_ref)
    zq = jnp.zeros((32, BQ), BF16)

    def block(step, _):
        hook(step)
        b = NB - 1 - step
        qs = pl.multiple_of(b * BQ, BQ)
        qcols = pl.ds(qs, BQ)
        last = b // 2
        q1T = rotT_ref[0:32, qcols]
        q2T = rotT_ref[32:64, qcols]
        rhs1 = jnp.concatenate([zq, zq, q1T, zq], axis=0)
        rhs2 = jnp.concatenate([zq, zq, zq, q2T], axis=0)

        def scores(j):
            ks = pl.multiple_of(j * BK, BK)
            kk = rot_ref[pl.ds(ks, BK), :]
            return ks, mm(kk, rhs1), mm(kk, rhs2)

        def ph1(j, c):
            m1, m2 = c
            ks, s1, s2 = scores(j)
            e1_ref[pl.ds(ks, BK), :] = s1
            e2_ref[pl.ds(ks, BK), :] = s2
            return jnp.maximum(m1, fold(s1, jnp.max)), jnp.maximum(m2, fold(s2, jnp.max))

        neg = jnp.full((8, BQ), -jnp.inf, F32)
        m1, m2 = lax.fori_loop(0, last, ph1, (neg, neg))
        ks, s1, s2 = scores(last)
        mask = (ks + lax.broadcasted_iota(jnp.int32, (BK, BQ), 0)) <= (qs + lax.broadcasted_iota(jnp.int32, (BK, BQ), 1))
        s1 = jnp.where(mask, s1, -jnp.inf)
        s2 = jnp.where(mask, s2, -jnp.inf)
        e1_ref[pl.ds(ks, BK), :] = s1
        e2_ref[pl.ds(ks, BK), :] = s2
        m1 = jnp.max(jnp.maximum(m1, fold(s1, jnp.max)), axis=0, keepdims=True)
        m2 = jnp.max(jnp.maximum(m2, fold(s2, jnp.max)), axis=0, keepdims=True)

        def ph2(j, c):
            l1, l2 = c
            rows = pl.ds(pl.multiple_of(j * BK, BK), BK)
            e1 = jnp.exp2((e1_ref[rows, :] - m1) * c2)
            e2 = jnp.exp2((e2_ref[rows, :] - m2) * c2)
            e1_ref[rows, :] = e1
            e2_ref[rows, :] = e2
            return l1 + fold(e1, jnp.sum), l2 + fold(e2, jnp.sum)

        zero = jnp.zeros((8, BQ), F32)
        l1, l2 = lax.fori_loop(0, last + 1, ph2, (zero, zero))
        r1 = 1.0 / jnp.sum(l1, axis=0, keepdims=True)
        r2 = lam / jnp.sum(l2, axis=0, keepdims=True)

        def ph3(j, o):
            rows = pl.ds(pl.multiple_of(j * BK, BK), BK)
            mix = (e1_ref[rows, :] * r1 - e2_ref[rows, :] * r2).astype(BF16)
            mix_ref[rows, :] = mix
            return o + mm(vgT_ref[0:64, rows], mix)

        o = lax.fori_loop(0, last + 1, ph3, jnp.zeros((64, BQ), F32))
        g = vgT_ref[64:128, qcols].astype(F32)
        ns = lax.rsqrt(jnp.mean(o * o, axis=0, keepdims=True) + NORM_EPS)
        ob = ns * g - ns * ns * ns * o * jnp.mean(g * o, axis=0, keepdims=True)
        obT = ob.astype(BF16)
        obp = jnp.concatenate([jnp.zeros((64, BQ), F32), ob], axis=0).T.astype(BF16)
        obz = jnp.concatenate([obT, jnp.zeros((64, BQ), BF16)], axis=0)

        def ph4(j, c):
            d1, d2 = c
            rows = pl.ds(pl.multiple_of(j * BK, BK), BK)
            dp = mm(vg_ref[rows, :], obz)
            dp_ref[rows, :] = dp
            return d1 + fold(dp * e1_ref[rows, :], jnp.sum), d2 + fold(dp * e2_ref[rows, :], jnp.sum)

        d1, d2 = lax.fori_loop(0, last + 1, ph4, (zero, zero))
        r2n = -r2
        d1 = jnp.sum(d1, axis=0, keepdims=True) * r1
        d2 = jnp.sum(d2, axis=0, keepdims=True) * (1.0 / jnp.sum(l2, axis=0, keepdims=True))
        f1 = r1 * inv_root
        f2 = r2n * inv_root
        lane = lax.broadcasted_iota(jnp.int32, (BQ, 128), 1)
        qrows = rot_ref[qcols, :]
        zb = jnp.zeros_like(qrows)
        rhs = jnp.concatenate([jnp.where(lane < 32, qrows, zb), jnp.where((lane >= 32) & (lane < 64), qrows, zb), obp], axis=0)

        def ph5(j, c):
            a1, a2 = c
            rows = pl.ds(pl.multiple_of(j * BK, BK), BK)
            dp = dp_ref[rows, :]
            g1 = (e1_ref[rows, :] * f1 * (dp - d1)).astype(BF16)
            g2 = (e2_ref[rows, :] * f2 * (dp - d2)).astype(BF16)
            lhs = jnp.concatenate([g1, g2, mix_ref[rows, :]], axis=1)
            acc_ref[rows, :] += mm(lhs, rhs)
            return a1 + mm(rotT_ref[64:96, rows], g1), a2 + mm(rotT_ref[96:128, rows], g2)

        za = jnp.zeros((32, BQ), F32)
        a1, a2 = lax.fori_loop(0, last + 1, ph5, (za, za))
        dqT_ref[0:32, qcols] = a1
        dqT_ref[32:64, qcols] = a2
        return 0

    lax.fori_loop(0, NB, block, 0)


TOK = 160
HALF = 80
D = 2048
COLS = 1024
TRANS_B = (((1,), (1,)), ((), ()))
MESH = pl.DeviceIdType.MESH


def join(a, b):
    return jnp.concatenate([a[:, :64], b[:, :64]], axis=1), jnp.concatenate([a[:, 64:], b[:, 64:]], axis=1)


def kernel(factor, lam_ref, tok_ref, wq_ref, wk_ref, v_ref, g_ref, cosT, sinT,
           tg_ref, vgrad_ref, dwq_ref, dwk_ref,
           tokF, wqF, wkF, wh4, wpk, tabC, tabS, qkS, xf, vgpack, vgF, rot, rotT, vgT, dqT, acc, e1, e2, mix, dp,
           backT, bpack, bF, dwp, dwR, dwS, dwG,
           t1s, t1r, t2s, t2r, p1s, p1r, m1s, m1r, hs, hr, qs, qr,
           wsend, wrecv, psend, precv, asend, arecv, bsend, brecv, rsend, rrecv, gsend, grecv, lsem):
    sp = lax.axis_index("sp")
    dpi = lax.axis_index("dp")
    core = lax.rem(dpi, 2)
    z = lax.div(dpi, 2)
    mate = z * 2 + 1 - core
    y, x = lax.div(sp, 4), lax.rem(sp, 4)
    u = y * (1 - core) + x * core
    w = x * (1 - core) + y * core

    def spot(uu, ww):
        uu, ww = lax.rem(uu + 4, 4), lax.rem(ww + 4, 4)
        return 4 * (uu * (1 - core) + ww * core) + ww * (1 - core) + uu * core

    barrier = pltpu.get_barrier_semaphore()
    for d in range(1, 16):
        pl.semaphore_signal(barrier, inc=1, device_id={"sp": lax.rem(sp + d, 16)}, device_id_type=MESH)
        pl.semaphore_signal(barrier, inc=1, device_id={"dp": lax.rem(dpi + d, 16)}, device_id_type=MESH)

    pair = pl.ds(pl.multiple_of(lax.div(sp, 2) * 128, 128), 128)
    lo, hi = join(wq_ref[:, pair], wk_ref[:, pair])
    wpk[...] = jnp.where(lax.rem(sp, 2) == 0, lo, hi)

    for p in range(8):
        lanes = slice(p * 128, (p + 1) * 128)
        vgpack[2 * p], vgpack[2 * p + 1] = join(v_ref[:, lanes], g_ref[:, lanes])

    pl.semaphore_wait(barrier, 30)

    sends = []

    def send(src, dst, ss, rs, to):
        def make():
            return pltpu.make_async_remote_copy(src_ref=src(), dst_ref=dst(), send_sem=ss(), recv_sem=rs(), device_id=to(),
                                                device_id_type=MESH)
        make().start()
        sends.append(make)

    def arrive(dst, ss, rs):
        pltpu.make_async_remote_copy(src_ref=dst, dst_ref=dst, send_sem=ss, recv_sem=rs, device_id={"sp": sp},
                                     device_id_type=MESH).wait_recv()

    def rows_of(i, n, at=0, size=None):
        return pl.ds(pl.multiple_of(i * n + at, 16), size or n)

    def t1_go(d):
        return {"sp": spot(u, w + 1 - 2 * d)}

    def t1_part(d, i):
        back = 1 if i < 2 else 2
        half = d if i != 1 else 1 - d
        return rows_of(spot(u, w - back if d == 0 else w + back), TOK, half * HALF, HALF)

    def t1_send(d, i):
        if i < 2:
            half = d if i == 0 else 1 - d
            send(lambda: tok_ref.at[pl.ds(half * HALF, HALF)], lambda: tokF.at[rows_of(sp, TOK, half * HALF, HALF)],
                 lambda: t1s.at[d, i], lambda: t1r.at[d, i], lambda: t1_go(d))
        else:
            send(lambda: tokF.at[t1_part(d, 0)], lambda: tokF.at[t1_part(d, 0)], lambda: t1s.at[d, i], lambda: t1r.at[d, i], lambda: t1_go(d))

    def t1_wait(d, i):
        arrive(tokF.at[t1_part(d, i)], t1s.at[d, i], t1r.at[d, i])

    def t2_go(d):
        return {"sp": spot(u + 1 - 2 * d, w)}

    def t2_rows(d, back, i, whole):
        b = spot(u - back if d == 0 else u + back, w + i)
        return rows_of(b, TOK) if whole else rows_of(b, TOK, d * HALF, HALF)

    def t2_send(d, i):
        send(lambda: tokF.at[t2_rows(d, 0, i, True)], lambda: tokF.at[t2_rows(d, 0, i, True)],
             lambda: t2s.at[d, i], lambda: t2r.at[d, i], lambda: t2_go(d))

    def t2_event(i):
        for d in range(2):
            arrive(tokF.at[t2_rows(d, 1, i, True)], t2s.at[d, i], t2r.at[d, i])
            send(lambda d=d: tokF.at[t2_rows(d, 1, i, False)], lambda d=d: tokF.at[t2_rows(d, 1, i, False)],
                 lambda d=d: t2s.at[d, 4 + i], lambda d=d: t2r.at[d, 4 + i], lambda d=d: t2_go(d))

    def t2_end():
        for i in range(4):
            for d in range(2):
                arrive(tokF.at[t2_rows(d, 2, i, False)], t2s.at[d, 4 + i], t2r.at[d, 4 + i])

    def lane_block(i):
        return pl.ds(pl.multiple_of(i * 128, 128), 128)

    def p1_send():
        for d in range(1, 8):
            send(lambda: wpk, lambda: wh4.at[rows_of(dpi, 128), lane_block(u)], lambda d=d: p1s.at[d], lambda d=d: p1r.at[d],
                 lambda d=d: {"dp": lax.rem(z + d, 8) * 2 + core})
        send(lambda: wpk, lambda: wh4.at[rows_of(dpi, 128), lane_block(w)], lambda: m1s.at[0], lambda: m1r.at[0], lambda: {"dp": mate})

    def p1_wait():
        for d in (1, 7, 2, 6, 3, 5, 4):
            part = lambda d=d: wh4.at[rows_of(lax.rem(z + 8 - d, 8) * 2 + core, 128), lane_block(u)]
            to = lambda d=d: wh4.at[rows_of(lax.rem(z + 8 - d, 8) * 2 + core, 128), lane_block(w)]
            arrive(part(), p1s.at[d], p1r.at[d])
            send(part, to, lambda d=d: m1s.at[d], lambda d=d: m1r.at[d], lambda: {"dp": mate})
        for d in range(8):
            arrive(wh4.at[rows_of(lax.rem(z + 8 - d, 8) * 2 + 1 - core, 128), lane_block(u)], m1s.at[d], m1r.at[d])

    def h_part(back, d, half):
        return wh4.at[pl.ds(half * 1024, 1024), lane_block(lax.rem(u + 4 - back if d == 0 else u + back, 4))]

    def h_send(d, i):
        half = d if i != 1 else 1 - d
        part = lambda: h_part(0 if i < 2 else 1, d, half)
        send(part, part, lambda: hs.at[d, i], lambda: hr.at[d, i], lambda: t2_go(d))

    def h_wait(d, i):
        arrive(h_part(1 if i < 2 else 2, d, d if i != 1 else 1 - d), hs.at[d, i], hr.at[d, i])

    wF = (wqF, wkF)
    wown = (wq_ref, wk_ref)

    def w_go(d):
        return {"dp": lax.rem(z + 1 + 6 * d, 8) * 2 + core}

    def w_owner(back, d):
        return lax.rem(z + 8 - back if d == 0 else z + back, 8) * 2 + core

    def w_which(d, k):
        return d if k == 6 else k % 2

    def w_send(d, k):
        m = w_which(d, k)
        send(lambda: wown[m] if k < 2 else wF[m].at[rows_of(w_owner(k // 2, d), 128)], lambda: wF[m].at[rows_of(w_owner(k // 2, d), 128)],
             lambda: wsend.at[d, k], lambda: wrecv.at[d, k], lambda: w_go(d))

    def mate_own(m):
        send(lambda: wown[m], lambda: wF[m].at[rows_of(dpi, 128)], lambda: psend.at[14 + m], lambda: precv.at[14 + m], lambda: {"dp": mate})

    def w_event(k):
        for d in range(2):
            m = w_which(d, k)
            part = lambda m=m, d=d: wF[m].at[rows_of(w_owner(k // 2 + 1, d), 128)]
            arrive(part(), wsend.at[d, k], wrecv.at[d, k])
            if k < 4 or k == 4 + d:
                w_send(d, k + 2 if k < 4 else 6)
            send(part, part, lambda d=d: psend.at[d * 7 + k], lambda d=d: precv.at[d * 7 + k], lambda: {"dp": mate})

    def mate_end():
        for m in range(2):
            arrive(wF[m].at[rows_of(mate, 128)], psend.at[14 + m], precv.at[14 + m])
        for k in range(7):
            for d in range(2):
                arrive(wF[w_which(d, k)].at[rows_of(w_owner(k // 2 + 1, d) + 1 - 2 * core, 128)], psend.at[d * 7 + k], precv.at[d * 7 + k])

    def vg_send():
        for d in range(1, 16):
            send(lambda d=d: vgpack.at[lax.rem(sp + d, 16)], lambda: vgF.at[rows_of(sp, TOK)], lambda d=d: asend.at[d], lambda d=d: arecv.at[d],
                 lambda d=d: {"sp": lax.rem(sp + d, 16)})

    def vg_wait():
        for d in range(1, 16):
            arrive(vgF.at[rows_of(lax.rem(sp + 16 - d, 16), TOK)], asend.at[d], arecv.at[d])

    def qk_send():
        for du in range(1, 4):
            for i in range(4):
                send(lambda du=du, i=i: qkS.at[lax.rem(u + du, 4), i], lambda i=i: rot.at[rows_of(spot(u, w + i), TOK)],
                     lambda du=du, i=i: qs.at[du, i], lambda du=du, i=i: qr.at[du, i], lambda du=du: {"sp": spot(u + du, w)})

    def qk_wait():
        for du in range(1, 4):
            for i in range(4):
                arrive(rot.at[rows_of(spot(u - du, w + i), TOK)], qs.at[du, i], qr.at[du, i])

    for i in range(2):
        for d in range(2):
            t1_send(d, i)
    p1_send()
    own = [pltpu.make_async_copy(tok_ref, tokF.at[rows_of(sp, TOK)], lsem.at[0]),
           pltpu.make_async_copy(wq_ref, wqF.at[rows_of(dpi, 128)], lsem.at[1]),
           pltpu.make_async_copy(wk_ref, wkF.at[rows_of(dpi, 128)], lsem.at[2])]
    for c in own:
        c.start()
    wh4[rows_of(dpi, 128), lane_block(u)] = wpk[...]
    vgF[rows_of(sp, TOK), :] = vgpack[sp]

    def tables(i, _):
        cols = pl.ds(pl.multiple_of(i * 128, 128), 128)
        c, s = cosT[:, cols], sinT[:, cols]
        tabC[cols, :] = jnp.concatenate([c] * 8, axis=0).T
        tabS[cols, :] = jnp.concatenate([-s, s] * 4, axis=0).T
        return 0
    lax.fori_loop(0, SEQ // 128, tables, 0)
    for c in own:
        c.wait()

    for d in range(2):
        t1_wait(d, 0)
        t1_send(d, 2)
    p1_wait()
    for i in range(2):
        for d in range(2):
            h_send(d, i)
    for k in range(2):
        for d in range(2):
            w_send(d, k)
    for m in range(2):
        mate_own(m)
    for d in range(2):
        t1_wait(d, 1)
        t1_wait(d, 2)
    for d in range(2):
        h_wait(d, 0)
        h_send(d, 2)
    vg_send()
    for d in range(2):
        h_wait(d, 1)
        h_wait(d, 2)

    lane16 = lax.rem(lax.broadcasted_iota(jnp.int32, (TOK, 128), 1), 32) < 16

    def project(i, _):
        b = spot(u, w + i)
        rows = rows_of(b, TOK)
        r = mm(tokF[rows, :], wh4[...])
        c, s = tabC[rows, :], tabS[rows, :]
        for h in range(4):
            a = r[:, h * 128:(h + 1) * 128]
            other = jnp.where(lane16, pltpu.roll(a, 112, 1), pltpu.roll(a, 16, 1))
            qkS[h, i] = (a * c + other * s).astype(BF16)
        return 0
    lax.fori_loop(0, 4, project, 0)
    for i in range(4):
        rot[rows_of(spot(u, w + i), TOK), :] = qkS[u, i]
    qk_send()
    for i in range(4):
        for d in range(2):
            t2_send(d, i)
    w_event(0)
    w_event(1)
    vg_wait()

    def turn_vg(i, _):
        r = pl.multiple_of(i * 256, 256)
        vgT[:, pl.ds(r, 256)] = vgF[pl.ds(r, 256), :].astype(F32).T.astype(BF16)
        return 0
    lax.fori_loop(0, SEQ // 256, turn_vg, 0)
    w_event(2)
    qk_wait()

    def turn_qk(i, _):
        r = pl.multiple_of(i * 256, 256)
        rotT[:, pl.ds(r, 256)] = rot[pl.ds(r, 256), :].astype(F32).T.astype(BF16)
        return 0
    lax.fori_loop(0, SEQ // 256, turn_qk, 0)

    def hook(step):
        plan = {0: [lambda: w_event(3)], 1: [lambda: t2_event(0), lambda: w_event(4)], 2: [lambda: t2_event(1), lambda: w_event(5)],
                3: [lambda: t2_event(2), lambda: w_event(6)], 4: [lambda: t2_event(3)]}
        for s, jobs in plan.items():
            @pl.when(step == s)
            def _():
                for j in jobs:
                    j()

    attention(lam_ref[sp], rot, rotT, vgF, vgT, cosT, sinT, dqT, acc, e1, e2, mix, dp, hook)

    def fin(i, _):
        cols = pl.ds(pl.multiple_of(i * 256, 256), 256)
        kvT = acc[cols, :].T
        c, s = cosT[:, cols], sinT[:, cols]
        bt = jnp.concatenate([rot_t(dqT[:, cols], c, s, -1.0), rot_t(kvT[0:64], c, s, -1.0)], axis=0)
        backT[:, cols] = bt.astype(BF16)
        xf[cols, :] = bt.T
        return 0
    lax.fori_loop(0, SEQ // 256, fin, 0)

    def pack(i, _):
        r = pl.multiple_of(i * TOK, TOK)
        bpack[i, 0:TOK, :] = xf[pl.ds(r, TOK), :].astype(BF16)
        dv0 = acc[pl.ds(r, HALF), :]
        dv1 = acc[pl.ds(r + HALF, HALF), :]
        bpack[i, TOK:TOK + HALF, :] = jnp.concatenate([dv0[:, 64:], dv1[:, 64:]], axis=1).astype(BF16)
        return 0
    lax.fori_loop(0, 16, pack, 0)
    bF[sp] = bpack[sp]
    t2_end()
    mate_end()

    def dw(i, _):
        cols = pl.ds(pl.multiple_of(i * 256, 256), 256)
        r = mm(backT[...], tokF[:, cols]).astype(BF16)
        dwp[2 * i] = r[:, :128]
        dwp[2 * i + 1] = r[:, 128:]
        return 0
    lax.fori_loop(0, 8, dw, 0)

    for d in range(1, 16):
        send(lambda d=d: bpack.at[lax.rem(sp + d, 16)], lambda: bF.at[sp], lambda d=d: bsend.at[d], lambda d=d: brecv.at[d],
             lambda d=d: {"sp": lax.rem(sp + d, 16)})
    for d in range(1, 16):
        send(lambda d=d: dwp.at[lax.rem(dpi + d, 16)], lambda: dwR.at[dpi], lambda d=d: rsend.at[d], lambda d=d: rrecv.at[d],
             lambda d=d: {"dp": lax.rem(dpi + d, 16)})
    dwR[dpi] = dwp[dpi]

    for d in range(1, 16):
        arrive(dwR.at[lax.rem(dpi + 16 - d, 16)], rsend.at[d], rrecv.at[d])
    total = dwR[0].astype(F32)
    for i in range(1, 16):
        total += dwR[i].astype(F32)
    dwS[...] = total.T.astype(BF16)
    dwG[sp] = total.T.astype(BF16)
    for d in range(1, 16):
        arrive(bF.at[lax.rem(sp + 16 - d, 16)], bsend.at[d], brecv.at[d])
    for d in range(1, 16):
        send(lambda: dwS, lambda: dwG.at[sp], lambda d=d: gsend.at[d], lambda d=d: grecv.at[d], lambda d=d: {"sp": lax.rem(sp + d, 16)})

    bq, bk = [], []
    for p in range(8):
        lanes = slice(p * 128, (p + 1) * 128)
        a, b = bF[2 * p], bF[2 * p + 1]
        q, k = join(a[:TOK], b[:TOK])
        bq.append(q)
        bk.append(k)
        top, low = join(a[TOK:], b[TOK:])
        vgrad_ref[0:HALF, lanes] = top
        vgrad_ref[HALF:TOK, lanes] = low
    bq = jnp.concatenate(bq, axis=1)
    bk = jnp.concatenate(bk, axis=1)
    for n in range(8):
        rows = slice(n * 256, (n + 1) * 256)
        tg_ref[:, rows] = (mm(bq, wqF[rows, :], TRANS_B) + mm(bk, wkF[rows, :], TRANS_B)).astype(BF16)

    for d in range(1, 16):
        arrive(dwG.at[lax.rem(sp + 16 - d, 16)], gsend.at[d], grecv.at[d])
    for p in range(8):
        lanes = slice(p * 128, (p + 1) * 128)
        q, k = join(dwG[2 * p].astype(F32), dwG[2 * p + 1].astype(F32))
        dwq_ref[:, lanes] = q * factor
        dwk_ref[:, lanes] = k * factor
    for make in sends:
        make().wait_send()


def body(tokens, query_weight, key_weight, values, lambdas, out_grad):
    half = DQK // 2
    freqs = jnp.exp(-math.log(THETA) * jnp.arange(half, dtype=F32) / half)
    angles = freqs[:, None] * jnp.arange(SEQ, dtype=jnp.int32).astype(F32)[None, :]
    vm = pl.BlockSpec(memory_space=pltpu.VMEM)
    dma = pltpu.SemaphoreType.DMA
    V = pltpu.VMEM
    return_shapes = (
        jax.ShapeDtypeStruct((TOK, D), BF16),
        jax.ShapeDtypeStruct((TOK, COLS), BF16),
        jax.ShapeDtypeStruct((128, COLS), F32),
        jax.ShapeDtypeStruct((128, COLS), F32),
    )
    tg, vg, dq, dk = pl.pallas_call(
        functools.partial(kernel, 1.0 / math.sqrt(16 * SEQ)),
        out_shape=return_shapes,
        in_specs=[pl.BlockSpec(memory_space=pltpu.SMEM)] + [vm] * 7,
        out_specs=(vm,) * 4,
        scratch_shapes=[
            V((SEQ, D), BF16), V((D, COLS), BF16), V((D, COLS), BF16), V((D, 512), BF16), V((128, 128), BF16),
            V((SEQ, 128), F32), V((SEQ, 128), F32), V((4, 4, TOK, 128), BF16), V((SEQ, 128), F32),
            V((16, TOK, 128), BF16), V((SEQ, 128), BF16),
            V((SEQ, 128), BF16), V((128, SEQ), BF16), V((128, SEQ), BF16), V((64, SEQ), F32), V((SEQ, 128), F32),
            V((SEQ, BQ), F32), V((SEQ, BQ), F32), V((SEQ, BQ), BF16), V((SEQ, BQ), F32),
            V((128, SEQ), BF16), V((16, TOK + HALF, 128), BF16), V((16, TOK + HALF, 128), BF16),
            V((16, 128, 128), BF16), V((16, 128, 128), BF16), V((128, 128), BF16), V((16, 128, 128), BF16),
            dma((2, 3)), dma((2, 3)), dma((2, 8)), dma((2, 8)), dma((8,)), dma((8,)), dma((8,)), dma((8,)),
            dma((2, 3)), dma((2, 3)), dma((4, 4)), dma((4, 4)),
            dma((2, 7)), dma((2, 7)), dma((16,)), dma((16,)), dma((16,)), dma((16,)),
            dma((16,)), dma((16,)), dma((16,)), dma((16,)), dma((16,)), dma((16,)), dma((3,)),
        ],
        compiler_params=pltpu.CompilerParams(vmem_limit_bytes=62 * 1024 * 1024, collective_id=0, has_side_effects=True),
        name="differential_backward",
    )(lambdas, tokens[0], query_weight, key_weight, values[0], out_grad[0], jnp.cos(angles), jnp.sin(angles))
    return tg[None], vg[None], dq, dk


def solution(mesh):
    in_specs = (
        P("dp", "sp", None),
        P("dp", None),
        P("dp", None),
        P("dp", "sp", None),
        P(),
        P("dp", "sp", None),
    )
    out_specs = (P("dp", "sp", None), P("dp", "sp", None), P("dp", None), P("dp", None))
    return jax.shard_map(body, mesh=mesh, in_specs=in_specs, out_specs=out_specs, check_vma=False)
```

time: 159 us -> 140 us (0.88)
  Pallas kernels: 151 us -> 132 us
    pallas_call x1, Pallas kernels: 151 us -> 132 us  [body(): pl.pallas_call(functools.partial(kernel, 1.0 / math.sqrt(16 * SEQ)), out_...]
where the time goes in v2:
time: 140 us
  Pallas kernels  132 us (94%)
  local copies, waits for them, and re-layouts  5.21 us (4%)
    pallas_call x1, Pallas kernels, body(): pl.pallas_call(functools.partial(kernel, 1.0 / math.sqrt(16 * SEQ)), out_...  132 us
    unnamed x10, local copies, waits for them, and re-layouts  5.21 us

profile of v2, /device:TPU:1, one launch (start us, length us, event | category | flops | bytes accessed | tf_op | source)
XLA Modules:
  0.0 139.6 jit_solution(11913570714195267834)
XLA Ops:
  0.7 1.4 multiply_sine_fusion
  2.0 132.3 %differential_backward.1 = (bf16[160,2048]{1,0:T(8,128)(2,1)}, bf16[160,1024]{1,0:T(8,128)(2,1)}, f32[128,1024]{1,0:T(8,128)}, f32[128,1024]{1,0:T(8,128)}) custom-call(f32[16]{0:T(128)} %lam_ref.1, bf16[160,2048]{1,0:T(8,128)(2,1)} %bitcast.5, bf16[128,1024]{1,0:T(8,128)(2,1)} %wq_ref.1, bf16[128,1024]{1,0:T(8,128)(2,1)} %wk_ref.1, ...), custom_call_target="tpu_custom_call" | custom-call | tf_op jit(solution)/shard_map/differential_backward/pallas_call | solution.py:514
  134.4 0.0 copy-start.2
  134.4 2.0 %copy.14 = bf16[1,160,2048]{2,1,0:T(8,128)(2,1)} copy(bf16[1,160,2048]{2,1,0:T(8,128)(2,1)} %bitcast.6) | data formatting | bytes 1310720
  136.4 0.0 copy-done.2
  136.4 0.0 copy-start.1
  136.4 0.7 copy.15
  137.1 0.4 copy-done.1
  137.6 0.0 copy-start
  137.6 0.8 copy.16
  138.4 0.4 copy-done
  138.8 0.8 copy.17
  (2 shorter events, 0.0 us)
Async XLA Ops:
  134.4 2.0 %copy-start.2 = (bf16[160,1024]{1,0:T(8,128)(2,1)S(1)}, bf16[160,1024]{1,0:T(8,128)(2,1)}, u32[]{:S(2)}) copy-start(bf16[160,1024]{1,0:T(8,128)(2,1)} %get-tuple-element.9) | copy-start | bytes 983044
  136.4 1.2 copy-start.1
  137.6 1.2 copy-start

commit v3 on v2

--- a/solution.py
+++ b/solution.py
@@ -3,6 +3,7 @@
 
 import jax
 import jax.numpy as jnp
+import numpy as np
 from jax import lax
 from jax.experimental import pallas as pl
 from jax.experimental.pallas import tpu as pltpu
@@ -13,7 +14,7 @@
 NORM_EPS = 0.1
 F32, BF16 = jnp.float32, jnp.bfloat16
 SEQ = 2560
-BQ = 256
+BQ = 512
 BK = 512
 NB = SEQ // BQ
 
@@ -35,18 +36,18 @@
     return op(r, axis=0)
 
 
-def attention(lam, rot_ref, rotT_ref, vg_ref, vgT_ref, cosT, sinT, dqT_ref, acc_ref, e1_ref, e2_ref, mix_ref, dp_ref, hook):
+def attention(lam, rot_ref, rotT_ref, vg_ref, vgT_ref, cosT, sinT, dqT_ref, acc_ref, e1_ref, e2_ref, mix_ref, dp_ref, hook, done):
     inv_root = 1.0 / math.sqrt(32)
     c2 = inv_root * math.log2(math.e)
     acc_ref[...] = jnp.zeros_like(acc_ref)
     zq = jnp.zeros((32, BQ), BF16)
 
     def block(step, _):
-        hook(step)
+        hook(step, 0)
         b = NB - 1 - step
         qs = pl.multiple_of(b * BQ, BQ)
         qcols = pl.ds(qs, BQ)
-        last = b // 2
+        last = b
         q1T = rotT_ref[0:32, qcols]
         q2T = rotT_ref[32:64, qcols]
         rhs1 = jnp.concatenate([zq, zq, q1T, zq], axis=0)
@@ -96,6 +97,7 @@
             return o + mm(vgT_ref[0:64, rows], mix)
 
         o = lax.fori_loop(0, last + 1, ph3, jnp.zeros((64, BQ), F32))
+        hook(step, 1)
         g = vgT_ref[64:128, qcols].astype(F32)
         ns = lax.rsqrt(jnp.mean(o * o, axis=0, keepdims=True) + NORM_EPS)
         ob = ns * g - ns * ns * ns * o * jnp.mean(g * o, axis=0, keepdims=True)
@@ -135,6 +137,7 @@
         a1, a2 = lax.fori_loop(0, last + 1, ph5, (za, za))
         dqT_ref[0:32, qcols] = a1
         dqT_ref[32:64, qcols] = a2
+        done(step, b)
         return 0
 
     lax.fori_loop(0, NB, block, 0)
@@ -152,10 +155,10 @@
     return jnp.concatenate([a[:, :64], b[:, :64]], axis=1), jnp.concatenate([a[:, 64:], b[:, 64:]], axis=1)
 
 
-def kernel(factor, lam_ref, tok_ref, wq_ref, wk_ref, v_ref, g_ref, cosT, sinT,
-           tg_ref, vgrad_ref, dwq_ref, dwk_ref,
+def kernel(lam_ref, tok_ref, wq_ref, wk_ref, v_ref, g_ref, cosT, sinT,
+           tg_ref, vgrad_ref, dw_ref,
            tokF, wqF, wkF, wh4, wpk, tabC, tabS, qkS, xf, vgpack, vgF, rot, rotT, vgT, dqT, acc, e1, e2, mix, dp,
-           backT, bpack, bF, dwp, dwR, dwS, dwG,
+           backT, bpack, bF, dwp, dwM, dwP, dwR, dwS, dwG,
            t1s, t1r, t2s, t2r, p1s, p1r, m1s, m1r, hs, hr, qs, qr,
            wsend, wrecv, psend, precv, asend, arecv, bsend, brecv, rsend, rrecv, gsend, grecv, lsem):
     sp = lax.axis_index("sp")
@@ -188,12 +191,12 @@
 
     sends = []
 
-    def send(src, dst, ss, rs, to):
+    def send(src, dst, ss, rs, to, when=None):
         def make():
             return pltpu.make_async_remote_copy(src_ref=src(), dst_ref=dst(), send_sem=ss(), recv_sem=rs(), device_id=to(),
                                                 device_id_type=MESH)
         make().start()
-        sends.append(make)
+        sends.append((make, when))
 
     def arrive(dst, ss, rs):
         pltpu.make_async_remote_copy(src_ref=dst, dst_ref=dst, send_sem=ss, recv_sem=rs, device_id={"sp": sp},
@@ -224,24 +227,28 @@
     def t2_go(d):
         return {"sp": spot(u + 1 - 2 * d, w)}
 
-    def t2_rows(d, back, i, whole):
-        b = spot(u - back if d == 0 else u + back, w + i)
-        return rows_of(b, TOK) if whole else rows_of(b, TOK, d * HALF, HALF)
-
-    def t2_send(d, i):
-        send(lambda: tokF.at[t2_rows(d, 0, i, True)], lambda: tokF.at[t2_rows(d, 0, i, True)],
-             lambda: t2s.at[d, i], lambda: t2r.at[d, i], lambda: t2_go(d))
+    def t2_rows(d, back, i, half):
+        return rows_of(spot(u - back if d == 0 else u + back, w + i), TOK, half * HALF, HALF)
+
+    def t2_send(d, i, k):
+        half = d if k != 1 else 1 - d
+        part = lambda: tokF.at[t2_rows(d, 1 if k == 2 else 0, i, half)]
+        src = (lambda: tok_ref.at[pl.ds(half * HALF, HALF)]) if i == 0 and k < 2 else part
+        send(src, part, lambda: t2s.at[d, i, k], lambda: t2r.at[d, i, k], lambda: t2_go(d))
+
+    def t2_wait(d, i, k):
+        arrive(tokF.at[t2_rows(d, 2 if k == 2 else 1, i, d if k != 1 else 1 - d)], t2s.at[d, i, k], t2r.at[d, i, k])
 
     def t2_event(i):
         for d in range(2):
-            arrive(tokF.at[t2_rows(d, 1, i, True)], t2s.at[d, i], t2r.at[d, i])
-            send(lambda d=d: tokF.at[t2_rows(d, 1, i, False)], lambda d=d: tokF.at[t2_rows(d, 1, i, False)],
-                 lambda d=d: t2s.at[d, 4 + i], lambda d=d: t2r.at[d, 4 + i], lambda d=d: t2_go(d))
+            t2_wait(d, i, 0)
+            t2_send(d, i, 2)
 
     def t2_end():
         for i in range(4):
             for d in range(2):
-                arrive(tokF.at[t2_rows(d, 2, i, False)], t2s.at[d, 4 + i], t2r.at[d, 4 + i])
+                t2_wait(d, i, 1)
+                t2_wait(d, i, 2)
 
     def lane_block(i):
         return pl.ds(pl.multiple_of(i * 128, 128), 128)
@@ -317,11 +324,10 @@
         for d in range(1, 16):
             arrive(vgF.at[rows_of(lax.rem(sp + 16 - d, 16), TOK)], asend.at[d], arecv.at[d])
 
-    def qk_send():
-        for du in range(1, 4):
-            for i in range(4):
-                send(lambda du=du, i=i: qkS.at[lax.rem(u + du, 4), i], lambda i=i: rot.at[rows_of(spot(u, w + i), TOK)],
-                     lambda du=du, i=i: qs.at[du, i], lambda du=du, i=i: qr.at[du, i], lambda du=du: {"sp": spot(u + du, w)})
+    def qk_send(i):
+        for du in (1, 3, 2):
+            send(lambda du=du: qkS.at[lax.rem(u + du, 4), i], lambda: rot.at[rows_of(spot(u, w + i), TOK)],
+                 lambda du=du: qs.at[du, i], lambda du=du: qr.at[du, i], lambda du=du: {"sp": spot(u + du, w)})
 
     def qk_wait():
         for du in range(1, 4):
@@ -332,6 +338,8 @@
         for d in range(2):
             t1_send(d, i)
     p1_send()
+    for d in range(2):
+        t2_send(d, 0, 0)
     own = [pltpu.make_async_copy(tok_ref, tokF.at[rows_of(sp, TOK)], lsem.at[0]),
            pltpu.make_async_copy(wq_ref, wqF.at[rows_of(dpi, 128)], lsem.at[1]),
            pltpu.make_async_copy(wk_ref, wkF.at[rows_of(dpi, 128)], lsem.at[2])]
@@ -370,28 +378,33 @@
         h_send(d, 2)
     vg_send()
     for d in range(2):
+        t2_send(d, 0, 1)
+    for d in range(2):
         h_wait(d, 1)
         h_wait(d, 2)
 
     lane16 = lax.rem(lax.broadcasted_iota(jnp.int32, (TOK, 128), 1), 32) < 16
 
-    def project(i, _):
-        b = spot(u, w + i)
-        rows = rows_of(b, TOK)
+    def project(i):
+        rows = rows_of(spot(u, w + i), TOK)
         r = mm(tokF[rows, :], wh4[...])
         c, s = tabC[rows, :], tabS[rows, :]
         for h in range(4):
             a = r[:, h * 128:(h + 1) * 128]
             other = jnp.where(lane16, pltpu.roll(a, 112, 1), pltpu.roll(a, 16, 1))
             qkS[h, i] = (a * c + other * s).astype(BF16)
-        return 0
-    lax.fori_loop(0, 4, project, 0)
+
+    for i in range(4):
+        project(i)
+        if i:
+            qk_send(i - 1)
     for i in range(4):
         rot[rows_of(spot(u, w + i), TOK), :] = qkS[u, i]
-    qk_send()
-    for i in range(4):
-        for d in range(2):
-            t2_send(d, i)
+    qk_send(3)
+    for i in range(1, 4):
+        for k in range(2):
+            for d in range(2):
+                t2_send(d, i, k)
     w_event(0)
     w_event(1)
     vg_wait()
@@ -402,6 +415,7 @@
         return 0
     lax.fori_loop(0, SEQ // 256, turn_vg, 0)
     w_event(2)
+    t2_event(0)
     qk_wait()
 
     def turn_qk(i, _):
@@ -410,66 +424,94 @@
         return 0
     lax.fori_loop(0, SEQ // 256, turn_qk, 0)
 
-    def hook(step):
-        plan = {0: [lambda: w_event(3)], 1: [lambda: t2_event(0), lambda: w_event(4)], 2: [lambda: t2_event(1), lambda: w_event(5)],
-                3: [lambda: t2_event(2), lambda: w_event(6)], 4: [lambda: t2_event(3)]}
-        for s, jobs in plan.items():
-            @pl.when(step == s)
-            def _():
-                for j in jobs:
-                    j()
-
-    attention(lam_ref[sp], rot, rotT, vgF, vgT, cosT, sinT, dqT, acc, e1, e2, mix, dp, hook)
-
-    def fin(i, _):
-        cols = pl.ds(pl.multiple_of(i * 256, 256), 256)
-        kvT = acc[cols, :].T
-        c, s = cosT[:, cols], sinT[:, cols]
-        bt = jnp.concatenate([rot_t(dqT[:, cols], c, s, -1.0), rot_t(kvT[0:64], c, s, -1.0)], axis=0)
-        backT[:, cols] = bt.astype(BF16)
-        xf[cols, :] = bt.T
-        return 0
-    lax.fori_loop(0, SEQ // 256, fin, 0)
-
-    def pack(i, _):
-        r = pl.multiple_of(i * TOK, TOK)
-        bpack[i, 0:TOK, :] = xf[pl.ds(r, TOK), :].astype(BF16)
-        dv0 = acc[pl.ds(r, HALF), :]
-        dv1 = acc[pl.ds(r + HALF, HALF), :]
-        bpack[i, TOK:TOK + HALF, :] = jnp.concatenate([dv0[:, 64:], dv1[:, 64:]], axis=1).astype(BF16)
-        return 0
-    lax.fori_loop(0, 16, pack, 0)
-    bF[sp] = bpack[sp]
+    batches = ((13, 14, 15), (10, 11, 12), (7, 8, 9), (4, 5, 6), (0, 1, 2, 3))
+
+    def back_one(j):
+        @pl.when(sp != j)
+        def _():
+            send(lambda: bpack.at[j], lambda: bF.at[sp], lambda: bsend.at[j], lambda: brecv.at[sp], lambda: {"sp": j}, lambda: sp != j)
+
+    def back_send(s):
+        for j in batches[s]:
+            back_one(j)
+
+    plan = {
+        (0, 0): [lambda: w_event(3)],
+        (0, 1): [lambda: t2_event(1)],
+        (1, 0): [lambda: w_event(4), lambda: back_send(0), lambda: t2_event(2)],
+        (1, 1): [lambda: w_event(5)],
+        (2, 0): [lambda: t2_event(3), lambda: back_send(1)],
+        (2, 1): [lambda: w_event(6)],
+        (3, 0): [lambda: back_send(2)],
+        (4, 0): [lambda: back_send(3)],
+    }
+
+    def hook(step, place):
+        for (s, p), jobs in plan.items():
+            if p == place:
+                @pl.when(step == s)
+                def _():
+                    for job in jobs:
+                        job()
+
+    def done(step, b):
+        for i in range(BQ // 256):
+            cols = pl.ds(pl.multiple_of(b * BQ + i * 256, 256), 256)
+            kvT = acc[cols, :].T
+            c, s = cosT[:, cols], sinT[:, cols]
+            bt = jnp.concatenate([rot_t(dqT[:, cols], c, s, -1.0), rot_t(kvT[0:64], c, s, -1.0)], axis=0)
+            backT[:, cols] = bt.astype(BF16)
+            xf[cols, :] = bt.T
+
+        first = jnp.where(step == NB - 1, 0, 13 - 3 * step)
+
+        def pack(k, _):
+            i = first + k
+            r = pl.multiple_of(i * TOK, TOK)
+            bpack[i, 0:TOK, :] = xf[pl.ds(r, TOK), :].astype(BF16)
+            dv0 = acc[pl.ds(r, HALF), :]
+            dv1 = acc[pl.ds(r + HALF, HALF), :]
+            bpack[i, TOK:TOK + HALF, :] = jnp.concatenate([dv0[:, 64:], dv1[:, 64:]], axis=1).astype(BF16)
+            return 0
+        lax.fori_loop(0, jnp.where(step == NB - 1, 4, 3), pack, 0)
+
+    attention(lam_ref[sp], rot, rotT, vgF, vgT, cosT, sinT, dqT, acc, e1, e2, mix, dp, hook, done)
+    back_send(4)
     t2_end()
-    mate_end()
 
     def dw(i, _):
         cols = pl.ds(pl.multiple_of(i * 256, 256), 256)
         r = mm(backT[...], tokF[:, cols]).astype(BF16)
-        dwp[2 * i] = r[:, :128]
-        dwp[2 * i + 1] = r[:, 128:]
+        dwp[0, i] = r[:, :128]
+        dwp[1, i] = r[:, 128:]
         return 0
     lax.fori_loop(0, 8, dw, 0)
-
+    bF[sp] = bpack[sp]
+    send(lambda: dwp.at[1 - core], lambda: dwM, lambda: rsend.at[8], lambda: rrecv.at[8], lambda: {"dp": mate})
+    mate_end()
+    arrive(dwM, rsend.at[8], rrecv.at[8])
+
+    def both(i, _):
+        dwP[i] = (dwp[core, i].astype(F32) + dwM[i].astype(F32)).astype(BF16)
+        return 0
+    lax.fori_loop(0, 8, both, 0)
+    for d in (4, 3, 5, 2, 6, 1, 7):
+        send(lambda d=d: dwP.at[lax.rem(z + d, 8)], lambda: dwR.at[z], lambda d=d: rsend.at[d], lambda d=d: rrecv.at[d],
+             lambda d=d: {"dp": lax.rem(z + d, 8) * 2 + core})
+    dwR[z] = dwP[z]
+    for d in range(1, 8):
+        arrive(dwR.at[lax.rem(z + 8 - d, 8)], rsend.at[d], rrecv.at[d])
+    total = dwR[0].astype(F32)
+    for i in range(1, 8):
+        total += dwR[i].astype(F32)
+    total = total.T.astype(BF16)
+    dwS[...] = total
+    dwG[sp] = total
+    for d in (10, 2, 8, 5, 7, 9, 11, 6, 14, 3, 13, 1, 4, 12, 15):
+        send(lambda: dwS, lambda: dwG.at[sp], lambda d=d: gsend.at[d], lambda d=d: grecv.at[d], lambda d=d: {"sp": lax.rem(sp + d, 16)})
     for d in range(1, 16):
-        send(lambda d=d: bpack.at[lax.rem(sp + d, 16)], lambda: bF.at[sp], lambda d=d: bsend.at[d], lambda d=d: brecv.at[d],
-             lambda d=d: {"sp": lax.rem(sp + d, 16)})
-    for d in range(1, 16):
-        send(lambda d=d: dwp.at[lax.rem(dpi + d, 16)], lambda: dwR.at[dpi], lambda d=d: rsend.at[d], lambda d=d: rrecv.at[d],
-             lambda d=d: {"dp": lax.rem(dpi + d, 16)})
-    dwR[dpi] = dwp[dpi]
-
-    for d in range(1, 16):
-        arrive(dwR.at[lax.rem(dpi + 16 - d, 16)], rsend.at[d], rrecv.at[d])
-    total = dwR[0].astype(F32)
-    for i in range(1, 16):
-        total += dwR[i].astype(F32)
-    dwS[...] = total.T.astype(BF16)
-    dwG[sp] = total.T.astype(BF16)
-    for d in range(1, 16):
-        arrive(bF.at[lax.rem(sp + 16 - d, 16)], bsend.at[d], brecv.at[d])
-    for d in range(1, 16):
-        send(lambda: dwS, lambda: dwG.at[sp], lambda d=d: gsend.at[d], lambda d=d: grecv.at[d], lambda d=d: {"sp": lax.rem(sp + d, 16)})
+        j = lax.rem(sp + d, 16)
+        arrive(bF.at[j], bsend.at[j], brecv.at[j])
 
     bq, bk = [], []
     for p in range(8):
@@ -489,33 +531,41 @@
 
     for d in range(1, 16):
         arrive(dwG.at[lax.rem(sp + 16 - d, 16)], gsend.at[d], grecv.at[d])
+    dw_ref[...] = dwG[...]
+    for make, when in sends:
+        if when is None:
+            make().wait_send()
+        else:
+            pl.when(when())(lambda make=make: make().wait_send())
+
+
+def settle(factor, tg_ref, vg_ref, dw_ref, tg_out, vg_out, dwq_out, dwk_out):
+    tg_out[...] = tg_ref[...]
+    vg_out[...] = vg_ref[...]
     for p in range(8):
         lanes = slice(p * 128, (p + 1) * 128)
-        q, k = join(dwG[2 * p].astype(F32), dwG[2 * p + 1].astype(F32))
-        dwq_ref[:, lanes] = q * factor
-        dwk_ref[:, lanes] = k * factor
-    for make in sends:
-        make().wait_send()
+        q, k = join(dw_ref[2 * p].astype(F32), dw_ref[2 * p + 1].astype(F32))
+        dwq_out[:, lanes] = q * factor
+        dwk_out[:, lanes] = k * factor
 
 
 def body(tokens, query_weight, key_weight, values, lambdas, out_grad):
     half = DQK // 2
-    freqs = jnp.exp(-math.log(THETA) * jnp.arange(half, dtype=F32) / half)
-    angles = freqs[:, None] * jnp.arange(SEQ, dtype=jnp.int32).astype(F32)[None, :]
+    freqs = np.exp(np.float32(-math.log(THETA)) * np.arange(half, dtype=np.float32) / np.float32(half))
+    angles = freqs[:, None] * np.arange(SEQ, dtype=np.float32)[None, :]
     vm = pl.BlockSpec(memory_space=pltpu.VMEM)
     dma = pltpu.SemaphoreType.DMA
     V = pltpu.VMEM
     return_shapes = (
         jax.ShapeDtypeStruct((TOK, D), BF16),
         jax.ShapeDtypeStruct((TOK, COLS), BF16),
-        jax.ShapeDtypeStruct((128, COLS), F32),
-        jax.ShapeDtypeStruct((128, COLS), F32),
+        jax.ShapeDtypeStruct((16, 128, 128), BF16),
     )
-    tg, vg, dq, dk = pl.pallas_call(
-        functools.partial(kernel, 1.0 / math.sqrt(16 * SEQ)),
+    raw = pl.pallas_call(
+        kernel,
         out_shape=return_shapes,
         in_specs=[pl.BlockSpec(memory_space=pltpu.SMEM)] + [vm] * 7,
-        out_specs=(vm,) * 4,
+        out_specs=(vm,) * 3,
         scratch_shapes=[
             V((SEQ, D), BF16), V((D, COLS), BF16), V((D, COLS), BF16), V((D, 512), BF16), V((128, 128), BF16),
             V((SEQ, 128), F32), V((SEQ, 128), F32), V((4, 4, TOK, 128), BF16), V((SEQ, 128), F32),
@@ -523,15 +573,23 @@
             V((SEQ, 128), BF16), V((128, SEQ), BF16), V((128, SEQ), BF16), V((64, SEQ), F32), V((SEQ, 128), F32),
             V((SEQ, BQ), F32), V((SEQ, BQ), F32), V((SEQ, BQ), BF16), V((SEQ, BQ), F32),
             V((128, SEQ), BF16), V((16, TOK + HALF, 128), BF16), V((16, TOK + HALF, 128), BF16),
-            V((16, 128, 128), BF16), V((16, 128, 128), BF16), V((128, 128), BF16), V((16, 128, 128), BF16),
-            dma((2, 3)), dma((2, 3)), dma((2, 8)), dma((2, 8)), dma((8,)), dma((8,)), dma((8,)), dma((8,)),
+            V((2, 8, 128, 128), BF16), V((8, 128, 128), BF16), V((8, 128, 128), BF16), V((8, 128, 128), BF16), V((128, 128), BF16), V((16, 128, 128), BF16),
+            dma((2, 3)), dma((2, 3)), dma((2, 4, 3)), dma((2, 4, 3)), dma((8,)), dma((8,)), dma((8,)), dma((8,)),
             dma((2, 3)), dma((2, 3)), dma((4, 4)), dma((4, 4)),
             dma((2, 7)), dma((2, 7)), dma((16,)), dma((16,)), dma((16,)), dma((16,)),
             dma((16,)), dma((16,)), dma((16,)), dma((16,)), dma((16,)), dma((16,)), dma((3,)),
         ],
         compiler_params=pltpu.CompilerParams(vmem_limit_bytes=62 * 1024 * 1024, collective_id=0, has_side_effects=True),
         name="differential_backward",
-    )(lambdas, tokens[0], query_weight, key_weight, values[0], out_grad[0], jnp.cos(angles), jnp.sin(angles))
+    )(lambdas, tokens[0], query_weight, key_weight, values[0], out_grad[0], jnp.asarray(np.cos(angles)), jnp.asarray(np.sin(angles)))
+    tg, vg, dq, dk = pl.pallas_call(
+        functools.partial(settle, 1.0 / math.sqrt(16 * SEQ)),
+        out_shape=(jax.ShapeDtypeStruct((TOK, D), BF16), jax.ShapeDtypeStruct((TOK, COLS), BF16),
+                   jax.ShapeDtypeStruct((128, COLS), F32), jax.ShapeDtypeStruct((128, COLS), F32)),
+        in_specs=[vm] * 3,
+        out_specs=(vm,) * 4,
+        name="settle",
+    )(*raw)
     return tg[None], vg[None], dq, dk
 
 

time: 140 us -> 126 us (0.900)
  Pallas kernels: 132 us -> 125 us
  local copies, waits for them, and re-layouts: 5.21 us -> 0 us
    pallas_call x1 -> x2, Pallas kernels: 132 us -> 125 us  [the longest x1 122 us: body(): pl.pallas_call(kernel, out_shape=return_shapes, in_specs=[pl.BlockSpec(me...]
    unnamed x10 -> x0, local copies, waits for them, and re-layouts: 5.21 us -> none
where the time goes in v3:
time: 126 us
  Pallas kernels  125 us (99%)
    pallas_call x1, Pallas kernels, body(): pl.pallas_call(kernel, out_shape=return_shapes, in_specs=[pl.BlockSpec(me...  122 us
    pallas_call x1, Pallas kernels, body(): pl.pallas_call(functools.partial(settle, 1.0 / math.sqrt(16 * SEQ)), out_...  2.83 us

profile of v3, /device:TPU:1, one launch (start us, length us, event | category | flops | bytes accessed | tf_op | source)
XLA Modules:
  0.0 125.7 jit_solution(16404040885142014130)
XLA Ops:
  0.6 122.3 %differential_backward.1 = (bf16[160,2048]{1,0:T(8,128)(2,1)}, bf16[160,1024]{1,0:T(8,128)(2,1)}, bf16[16,128,128]{2,1,0:T(8,128)(2,1)}) custom-call(f32[16]{0:T(128)} %lam_ref.1, bf16[160,2048]{1,0:T(8,128)(2,1)} %bitcast.5, bf16[128,1024]{1,0:T(8,128)(2,1)} %wq_ref.1, bf16[128,1024]{1,0:T(8,128)(2,1)} %wk_ref.1, bf16[160,1024]{1,0:T(8,128)(2,1)} %bitcast.6, ...), custom_call_target="tpu_custom_call" | custom-call | tf_op jit(solution)/shard_map/differential_backward/pallas_call | solution.py:564
  122.9 2.8 %settle.1 = (bf16[160,2048]{1,0:T(8,128)(2,1)}, bf16[160,1024]{1,0:T(8,128)(2,1)}, f32[128,1024]{1,0:T(8,128)}, f32[128,1024]{1,0:T(8,128)}) custom-call(bf16[160,2048]{1,0:T(8,128)(2,1)} %get-tuple-element.11.tg_ref, bf16[160,1024]{1,0:T(8,128)(2,1)} %get-tuple-element.12.vg_ref, bf16[16,128,128]{2,1,0:T(8,128)(2,1)} %get-tuple-element.13.dw_ref), custom_call_target="tpu_custom_call" | custom-call | tf_op jit(solution)/shard_map/settle/pallas_call | solution.py:585

commit v4 on v3

--- a/solution.py
+++ b/solution.py
@@ -36,10 +36,10 @@
     return op(r, axis=0)
 
 
-def attention(lam, rot_ref, rotT_ref, vg_ref, vgT_ref, cosT, sinT, dqT_ref, acc_ref, e1_ref, e2_ref, mix_ref, dp_ref, hook, done):
+def attention(lam, rot_ref, rotT_ref, vg_ref, vgT_ref, cosT, sinT, dqT_ref, accT_ref, e1_ref, e2_ref, mix_ref, dp_ref, hook, done):
     inv_root = 1.0 / math.sqrt(32)
     c2 = inv_root * math.log2(math.e)
-    acc_ref[...] = jnp.zeros_like(acc_ref)
+    accT_ref[...] = jnp.zeros_like(accT_ref)
     zq = jnp.zeros((32, BQ), BF16)
 
     def block(step, _):
@@ -129,8 +129,10 @@
             dp = dp_ref[rows, :]
             g1 = (e1_ref[rows, :] * f1 * (dp - d1)).astype(BF16)
             g2 = (e2_ref[rows, :] * f2 * (dp - d2)).astype(BF16)
-            lhs = jnp.concatenate([g1, g2, mix_ref[rows, :]], axis=1)
-            acc_ref[rows, :] += mm(lhs, rhs)
+            tb = (((1,), (1,)), ((), ()))
+            accT_ref[0:32, rows] += mm(q1T, g1, tb)
+            accT_ref[32:64, rows] += mm(q2T, g2, tb)
+            accT_ref[64:128, rows] += mm(obT, mix_ref[rows, :], tb)
             return a1 + mm(rotT_ref[64:96, rows], g1), a2 + mm(rotT_ref[96:128, rows], g2)
 
         za = jnp.zeros((32, BQ), F32)
@@ -157,7 +159,7 @@
 
 def kernel(lam_ref, tok_ref, wq_ref, wk_ref, v_ref, g_ref, cosT, sinT,
            tg_ref, vgrad_ref, dw_ref,
-           tokF, wqF, wkF, wh4, wpk, tabC, tabS, qkS, xf, vgpack, vgF, rot, rotT, vgT, dqT, acc, e1, e2, mix, dp,
+           tokF, wqF, wkF, wh4, wpk, tabC, tabS, qkS, xf, xv, vgpack, vgF, rot, rotT, vgT, dqT, acc, e1, e2, mix, dp,
            backT, bpack, bF, dwp, dwM, dwP, dwR, dwS, dwG,
            t1s, t1r, t2s, t2r, p1s, p1r, m1s, m1r, hs, hr, qs, qr,
            wsend, wrecv, psend, precv, asend, arecv, bsend, brecv, rsend, rrecv, gsend, grecv, lsem):
@@ -386,21 +388,22 @@
     lane16 = lax.rem(lax.broadcasted_iota(jnp.int32, (TOK, 128), 1), 32) < 16
 
     def project(i):
-        rows = rows_of(spot(u, w + i), TOK)
-        r = mm(tokF[rows, :], wh4[...])
-        c, s = tabC[rows, :], tabS[rows, :]
-        for h in range(4):
-            a = r[:, h * 128:(h + 1) * 128]
-            other = jnp.where(lane16, pltpu.roll(a, 112, 1), pltpu.roll(a, 16, 1))
-            qkS[h, i] = (a * c + other * s).astype(BF16)
-
-    for i in range(4):
-        project(i)
-        if i:
-            qk_send(i - 1)
+        rows = [rows_of(spot(u, w + i + n), TOK) for n in range(2)]
+        r = mm(jnp.concatenate([tokF[p, :] for p in rows], axis=0), wh4[...])
+        for n in range(2):
+            c, s = tabC[rows[n], :], tabS[rows[n], :]
+            for h in range(4):
+                a = r[n * TOK:(n + 1) * TOK, h * 128:(h + 1) * 128]
+                other = jnp.where(lane16, pltpu.roll(a, 112, 1), pltpu.roll(a, 16, 1))
+                qkS[h, i + n] = (a * c + other * s).astype(BF16)
+
+    project(0)
+    qk_send(0)
+    project(2)
+    for i in range(1, 4):
+        qk_send(i)
     for i in range(4):
         rot[rows_of(spot(u, w + i), TOK), :] = qkS[u, i]
-    qk_send(3)
     for i in range(1, 4):
         for k in range(2):
             for d in range(2):
@@ -414,7 +417,6 @@
         vgT[:, pl.ds(r, 256)] = vgF[pl.ds(r, 256), :].astype(F32).T.astype(BF16)
         return 0
     lax.fori_loop(0, SEQ // 256, turn_vg, 0)
-    w_event(2)
     t2_event(0)
     qk_wait()
 
@@ -424,26 +426,17 @@
         return 0
     lax.fori_loop(0, SEQ // 256, turn_qk, 0)
 
-    batches = ((13, 14, 15), (10, 11, 12), (7, 8, 9), (4, 5, 6), (0, 1, 2, 3))
-
-    def back_one(j):
-        @pl.when(sp != j)
-        def _():
-            send(lambda: bpack.at[j], lambda: bF.at[sp], lambda: bsend.at[j], lambda: brecv.at[sp], lambda: {"sp": j}, lambda: sp != j)
-
-    def back_send(s):
-        for j in batches[s]:
-            back_one(j)
+    def back_send():
+        for d in (10, 2, 8, 5, 7, 9, 11, 6, 14, 3, 13, 1, 4, 12, 15):
+            send(lambda d=d: bpack.at[lax.rem(sp + d, 16)], lambda: bF.at[sp], lambda d=d: bsend.at[d], lambda d=d: brecv.at[d],
+                 lambda d=d: {"sp": lax.rem(sp + d, 16)})
 
     plan = {
-        (0, 0): [lambda: w_event(3)],
-        (0, 1): [lambda: t2_event(1)],
-        (1, 0): [lambda: w_event(4), lambda: back_send(0), lambda: t2_event(2)],
-        (1, 1): [lambda: w_event(5)],
-        (2, 0): [lambda: t2_event(3), lambda: back_send(1)],
+        (0, 0): [lambda: w_event(2)],
+        (0, 1): [lambda: w_event(3), lambda: t2_event(1)],
+        (1, 0): [lambda: w_event(4), lambda: t2_event(2)],
+        (1, 1): [lambda: w_event(5), lambda: t2_event(3)],
         (2, 1): [lambda: w_event(6)],
-        (3, 0): [lambda: back_send(2)],
-        (4, 0): [lambda: back_send(3)],
     }
 
     def hook(step, place):
@@ -457,11 +450,11 @@
     def done(step, b):
         for i in range(BQ // 256):
             cols = pl.ds(pl.multiple_of(b * BQ + i * 256, 256), 256)
-            kvT = acc[cols, :].T
             c, s = cosT[:, cols], sinT[:, cols]
-            bt = jnp.concatenate([rot_t(dqT[:, cols], c, s, -1.0), rot_t(kvT[0:64], c, s, -1.0)], axis=0)
+            bt = jnp.concatenate([rot_t(dqT[:, cols], c, s, -1.0), rot_t(acc[0:64, cols], c, s, -1.0)], axis=0)
             backT[:, cols] = bt.astype(BF16)
             xf[cols, :] = bt.T
+            xv[cols, :] = acc[64:128, cols].T
 
         first = jnp.where(step == NB - 1, 0, 13 - 3 * step)
 
@@ -469,14 +462,12 @@
             i = first + k
             r = pl.multiple_of(i * TOK, TOK)
             bpack[i, 0:TOK, :] = xf[pl.ds(r, TOK), :].astype(BF16)
-            dv0 = acc[pl.ds(r, HALF), :]
-            dv1 = acc[pl.ds(r + HALF, HALF), :]
-            bpack[i, TOK:TOK + HALF, :] = jnp.concatenate([dv0[:, 64:], dv1[:, 64:]], axis=1).astype(BF16)
+            bpack[i, TOK:TOK + HALF, :] = jnp.concatenate([xv[pl.ds(r, HALF), :], xv[pl.ds(r + HALF, HALF), :]], axis=1).astype(BF16)
             return 0
         lax.fori_loop(0, jnp.where(step == NB - 1, 4, 3), pack, 0)
 
     attention(lam_ref[sp], rot, rotT, vgF, vgT, cosT, sinT, dqT, acc, e1, e2, mix, dp, hook, done)
-    back_send(4)
+    back_send()
     t2_end()
 
     def dw(i, _):
@@ -510,8 +501,7 @@
     for d in (10, 2, 8, 5, 7, 9, 11, 6, 14, 3, 13, 1, 4, 12, 15):
         send(lambda: dwS, lambda: dwG.at[sp], lambda d=d: gsend.at[d], lambda d=d: grecv.at[d], lambda d=d: {"sp": lax.rem(sp + d, 16)})
     for d in range(1, 16):
-        j = lax.rem(sp + d, 16)
-        arrive(bF.at[j], bsend.at[j], brecv.at[j])
+        arrive(bF.at[lax.rem(sp + 16 - d, 16)], bsend.at[d], brecv.at[d])
 
     bq, bk = [], []
     for p in range(8):
@@ -568,9 +558,9 @@
         out_specs=(vm,) * 3,
         scratch_shapes=[
             V((SEQ, D), BF16), V((D, COLS), BF16), V((D, COLS), BF16), V((D, 512), BF16), V((128, 128), BF16),
-            V((SEQ, 128), F32), V((SEQ, 128), F32), V((4, 4, TOK, 128), BF16), V((SEQ, 128), F32),
+            V((SEQ, 128), F32), V((SEQ, 128), F32), V((4, 4, TOK, 128), BF16), V((SEQ, 128), F32), V((SEQ, 64), F32),
             V((16, TOK, 128), BF16), V((SEQ, 128), BF16),
-            V((SEQ, 128), BF16), V((128, SEQ), BF16), V((128, SEQ), BF16), V((64, SEQ), F32), V((SEQ, 128), F32),
+            V((SEQ, 128), BF16), V((128, SEQ), BF16), V((128, SEQ), BF16), V((64, SEQ), F32), V((128, SEQ), F32),
             V((SEQ, BQ), F32), V((SEQ, BQ), F32), V((SEQ, BQ), BF16), V((SEQ, BQ), F32),
             V((128, SEQ), BF16), V((16, TOK + HALF, 128), BF16), V((16, TOK + HALF, 128), BF16),
             V((2, 8, 128, 128), BF16), V((8, 128, 128), BF16), V((8, 128, 128), BF16), V((8, 128, 128), BF16), V((128, 128), BF16), V((16, 128, 128), BF16),

time: 126 us -> 118 us (0.937)
  Pallas kernels: 125 us -> 117 us
    pallas_call x1, Pallas kernels: 122 us -> 115 us  [body(): pl.pallas_call(kernel, out_shape=return_shapes, in_specs=[pl.BlockSpec(me...]
where the time goes in v4:
time: 118 us
  Pallas kernels  117 us (99%)
    pallas_call x1, Pallas kernels, body(): pl.pallas_call(kernel, out_shape=return_shapes, in_specs=[pl.BlockSpec(me...  115 us
    pallas_call x1, Pallas kernels, body(): pl.pallas_call(functools.partial(settle, 1.0 / math.sqrt(16 * SEQ)), out_...  2.83 us

profile of v4, /device:TPU:1, one launch (start us, length us, event | category | flops | bytes accessed | tf_op | source)
XLA Modules:
  0.0 118.1 jit_solution(8799414910725059580)
XLA Ops:
  0.6 114.6 %differential_backward.1 = (bf16[160,2048]{1,0:T(8,128)(2,1)}, bf16[160,1024]{1,0:T(8,128)(2,1)}, bf16[16,128,128]{2,1,0:T(8,128)(2,1)}) custom-call(f32[16]{0:T(128)} %lam_ref.1, bf16[160,2048]{1,0:T(8,128)(2,1)} %bitcast.5, bf16[128,1024]{1,0:T(8,128)(2,1)} %wq_ref.1, bf16[128,1024]{1,0:T(8,128)(2,1)} %wk_ref.1, bf16[160,1024]{1,0:T(8,128)(2,1)} %bitcast.6, ...), custom_call_target="tpu_custom_call" | custom-call | tf_op jit(solution)/shard_map/differential_backward/pallas_call | solution.py:554
  115.3 2.8 %settle.1 = (bf16[160,2048]{1,0:T(8,128)(2,1)}, bf16[160,1024]{1,0:T(8,128)(2,1)}, f32[128,1024]{1,0:T(8,128)}, f32[128,1024]{1,0:T(8,128)}) custom-call(bf16[160,2048]{1,0:T(8,128)(2,1)} %get-tuple-element.11.tg_ref, bf16[160,1024]{1,0:T(8,128)(2,1)} %get-tuple-element.12.vg_ref, bf16[16,128,128]{2,1,0:T(8,128)(2,1)} %get-tuple-element.13.dw_ref), custom_call_target="tpu_custom_call" | custom-call | tf_op jit(solution)/shard_map/settle/pallas_call | solution.py:575

commit v5 on v4

--- a/solution.py
+++ b/solution.py
@@ -162,7 +162,7 @@
            tokF, wqF, wkF, wh4, wpk, tabC, tabS, qkS, xf, xv, vgpack, vgF, rot, rotT, vgT, dqT, acc, e1, e2, mix, dp,
            backT, bpack, bF, dwp, dwM, dwP, dwR, dwS, dwG,
            t1s, t1r, t2s, t2r, p1s, p1r, m1s, m1r, hs, hr, qs, qr,
-           wsend, wrecv, psend, precv, asend, arecv, bsend, brecv, rsend, rrecv, gsend, grecv, lsem):
+           wsend, wrecv, psend, precv, asend, arecv, bsend, brecv, rsend, rrecv, gsend, grecv, g2send, g2recv, lsem):
     sp = lax.axis_index("sp")
     dpi = lax.axis_index("dp")
     core = lax.rem(dpi, 2)
@@ -367,11 +367,6 @@
     for i in range(2):
         for d in range(2):
             h_send(d, i)
-    for k in range(2):
-        for d in range(2):
-            w_send(d, k)
-    for m in range(2):
-        mate_own(m)
     for d in range(2):
         t1_wait(d, 1)
         t1_wait(d, 2)
@@ -381,6 +376,11 @@
     vg_send()
     for d in range(2):
         t2_send(d, 0, 1)
+    for k in range(2):
+        for d in range(2):
+            w_send(d, k)
+    for m in range(2):
+        mate_own(m)
     for d in range(2):
         h_wait(d, 1)
         h_wait(d, 2)
@@ -409,7 +409,6 @@
             for d in range(2):
                 t2_send(d, i, k)
     w_event(0)
-    w_event(1)
     vg_wait()
 
     def turn_vg(i, _):
@@ -417,7 +416,6 @@
         vgT[:, pl.ds(r, 256)] = vgF[pl.ds(r, 256), :].astype(F32).T.astype(BF16)
         return 0
     lax.fori_loop(0, SEQ // 256, turn_vg, 0)
-    t2_event(0)
     qk_wait()
 
     def turn_qk(i, _):
@@ -432,11 +430,12 @@
                  lambda d=d: {"sp": lax.rem(sp + d, 16)})
 
     plan = {
-        (0, 0): [lambda: w_event(2)],
-        (0, 1): [lambda: w_event(3), lambda: t2_event(1)],
-        (1, 0): [lambda: w_event(4), lambda: t2_event(2)],
-        (1, 1): [lambda: w_event(5), lambda: t2_event(3)],
-        (2, 1): [lambda: w_event(6)],
+        (0, 0): [lambda: w_event(1)],
+        (0, 1): [lambda: w_event(2), lambda: t2_event(0)],
+        (1, 0): [lambda: w_event(3), lambda: t2_event(1)],
+        (1, 1): [lambda: w_event(4), lambda: t2_event(2)],
+        (2, 0): [lambda: w_event(5), lambda: t2_event(3)],
+        (3, 0): [lambda: w_event(6)],
     }
 
     def hook(step, place):
@@ -470,26 +469,36 @@
     back_send()
     t2_end()
 
-    def dw(i, _):
-        cols = pl.ds(pl.multiple_of(i * 256, 256), 256)
-        r = mm(backT[...], tokF[:, cols]).astype(BF16)
-        dwp[0, i] = r[:, :128]
-        dwp[1, i] = r[:, 128:]
-        return 0
-    lax.fori_loop(0, 8, dw, 0)
+    far = (4, 3, 5, 2, 6, 1, 7, 0)
+
+    def chip(i):
+        return lax.rem(z + far[i], 8)
+
+    def piece(i):
+        r = mm(backT[...], tokF[:, pl.ds(pl.multiple_of(chip(i) * 256, 256), 256)]).astype(BF16)
+        dwp[0, chip(i)] = r[:, :128]
+        dwp[1, chip(i)] = r[:, 128:]
+
+    def piece_mate(i):
+        send(lambda: dwp.at[1 - core, chip(i)], lambda: dwM.at[chip(i)], lambda: rsend.at[8 + i], lambda: rrecv.at[8 + i], lambda: {"dp": mate})
+
+    def piece_add(i):
+        arrive(dwM.at[chip(i)], rsend.at[8 + i], rrecv.at[8 + i])
+        both = (dwp[core, chip(i)].astype(F32) + dwM[chip(i)].astype(F32)).astype(BF16)
+        dwP[chip(i)] = both
+        if far[i] == 0:
+            dwR[z] = both
+
+    def piece_go(i):
+        if far[i]:
+            send(lambda: dwP.at[chip(i)], lambda: dwR.at[z], lambda: rsend.at[far[i]], lambda: rrecv.at[far[i]], lambda: {"dp": chip(i) * 2 + core})
+
+    for t in range(15):
+        for job, late in ((piece, 0), (piece_mate, 1), (piece_add, 5), (piece_go, 6)):
+            if 0 <= t - late < 8:
+                job(t - late)
     bF[sp] = bpack[sp]
-    send(lambda: dwp.at[1 - core], lambda: dwM, lambda: rsend.at[8], lambda: rrecv.at[8], lambda: {"dp": mate})
     mate_end()
-    arrive(dwM, rsend.at[8], rrecv.at[8])
-
-    def both(i, _):
-        dwP[i] = (dwp[core, i].astype(F32) + dwM[i].astype(F32)).astype(BF16)
-        return 0
-    lax.fori_loop(0, 8, both, 0)
-    for d in (4, 3, 5, 2, 6, 1, 7):
-        send(lambda d=d: dwP.at[lax.rem(z + d, 8)], lambda: dwR.at[z], lambda d=d: rsend.at[d], lambda d=d: rrecv.at[d],
-             lambda d=d: {"dp": lax.rem(z + d, 8) * 2 + core})
-    dwR[z] = dwP[z]
     for d in range(1, 8):
         arrive(dwR.at[lax.rem(z + 8 - d, 8)], rsend.at[d], rrecv.at[d])
     total = dwR[0].astype(F32)
@@ -498,8 +507,18 @@
     total = total.T.astype(BF16)
     dwS[...] = total
     dwG[sp] = total
-    for d in (10, 2, 8, 5, 7, 9, 11, 6, 14, 3, 13, 1, 4, 12, 15):
-        send(lambda: dwS, lambda: dwG.at[sp], lambda d=d: gsend.at[d], lambda d=d: grecv.at[d], lambda d=d: {"sp": lax.rem(sp + d, 16)})
+
+    def row_send(dw):
+        send(lambda: dwS, lambda: dwG.at[sp], lambda: gsend.at[dw], lambda: grecv.at[dw], lambda: {"sp": spot(u, w + dw)})
+
+    def column_send(i):
+        for du in (2, 1, 3):
+            send(lambda: dwS if i == 0 else dwG.at[spot(u, w - i)], lambda: dwG.at[spot(u, w - i)], lambda du=du: g2send.at[du, i],
+                 lambda du=du: g2recv.at[du, i], lambda du=du: {"sp": spot(u + du, w)})
+
+    for dw in (2, 1, 3):
+        row_send(dw)
+    column_send(0)
     for d in range(1, 16):
         arrive(bF.at[lax.rem(sp + 16 - d, 16)], bsend.at[d], brecv.at[d])
 
@@ -515,12 +534,16 @@
         vgrad_ref[HALF:TOK, lanes] = low
     bq = jnp.concatenate(bq, axis=1)
     bk = jnp.concatenate(bk, axis=1)
+    for i in (1, 3, 2):
+        arrive(dwG.at[spot(u, w - i)], gsend.at[i], grecv.at[i])
+        column_send(i)
     for n in range(8):
         rows = slice(n * 256, (n + 1) * 256)
         tg_ref[:, rows] = (mm(bq, wqF[rows, :], TRANS_B) + mm(bk, wkF[rows, :], TRANS_B)).astype(BF16)
 
-    for d in range(1, 16):
-        arrive(dwG.at[lax.rem(sp + 16 - d, 16)], gsend.at[d], grecv.at[d])
+    for i in range(4):
+        for du in range(1, 4):
+            arrive(dwG.at[spot(u - du, w - i)], g2send.at[du, i], g2recv.at[du, i])
     dw_ref[...] = dwG[...]
     for make, when in sends:
         if when is None:
@@ -567,7 +590,7 @@
             dma((2, 3)), dma((2, 3)), dma((2, 4, 3)), dma((2, 4, 3)), dma((8,)), dma((8,)), dma((8,)), dma((8,)),
             dma((2, 3)), dma((2, 3)), dma((4, 4)), dma((4, 4)),
             dma((2, 7)), dma((2, 7)), dma((16,)), dma((16,)), dma((16,)), dma((16,)),
-            dma((16,)), dma((16,)), dma((16,)), dma((16,)), dma((16,)), dma((16,)), dma((3,)),
+            dma((16,)), dma((16,)), dma((16,)), dma((16,)), dma((4,)), dma((4,)), dma((4, 4)), dma((4, 4)), dma((3,)),
         ],
         compiler_params=pltpu.CompilerParams(vmem_limit_bytes=62 * 1024 * 1024, collective_id=0, has_side_effects=True),
         name="differential_backward",

time: 118 us -> 115 us (0.975)
  Pallas kernels: 117 us -> 113 us
    pallas_call x1, Pallas kernels: 115 us -> 111 us  [body(): pl.pallas_call(kernel, out_shape=return_shapes, in_specs=[pl.BlockSpec(me...]
where the time goes in v5:
time: 115 us; the launch traced here: 114 us
  Pallas kernels  113 us (98%)
    pallas_call x1, Pallas kernels, body(): pl.pallas_call(kernel, out_shape=return_shapes, in_specs=[pl.BlockSpec(me...  111 us
    pallas_call x1, Pallas kernels, body(): pl.pallas_call(functools.partial(settle, 1.0 / math.sqrt(16 * SEQ)), out_...  2.83 us

profile of v5, /device:TPU:1, one launch (start us, length us, event | category | flops | bytes accessed | tf_op | source)
XLA Modules:
  0.0 114.1 jit_solution(13306178552138936361)
XLA Ops:
  0.6 110.6 %differential_backward.1 = (bf16[160,2048]{1,0:T(8,128)(2,1)}, bf16[160,1024]{1,0:T(8,128)(2,1)}, bf16[16,128,128]{2,1,0:T(8,128)(2,1)}) custom-call(f32[16]{0:T(128)} %lam_ref.1, bf16[160,2048]{1,0:T(8,128)(2,1)} %bitcast.5, bf16[128,1024]{1,0:T(8,128)(2,1)} %wq_ref.1, bf16[128,1024]{1,0:T(8,128)(2,1)} %wk_ref.1, bf16[160,1024]{1,0:T(8,128)(2,1)} %bitcast.6, ...), custom_call_target="tpu_custom_call" | custom-call | tf_op jit(solution)/shard_map/differential_backward/pallas_call | solution.py:577
  111.3 2.8 %settle.1 = (bf16[160,2048]{1,0:T(8,128)(2,1)}, bf16[160,1024]{1,0:T(8,128)(2,1)}, f32[128,1024]{1,0:T(8,128)}, f32[128,1024]{1,0:T(8,128)}) custom-call(bf16[160,2048]{1,0:T(8,128)(2,1)} %get-tuple-element.11.tg_ref, bf16[160,1024]{1,0:T(8,128)(2,1)} %get-tuple-element.12.vg_ref, bf16[16,128,128]{2,1,0:T(8,128)(2,1)} %get-tuple-element.13.dw_ref), custom_call_target="tpu_custom_call" | custom-call | tf_op jit(solution)/shard_map/settle/pallas_call | solution.py:598

commit v6 on v5

--- a/solution.py
+++ b/solution.py
@@ -466,8 +466,8 @@
         lax.fori_loop(0, jnp.where(step == NB - 1, 4, 3), pack, 0)
 
     attention(lam_ref[sp], rot, rotT, vgF, vgT, cosT, sinT, dqT, acc, e1, e2, mix, dp, hook, done)
+    t2_end()
     back_send()
-    t2_end()
 
     far = (4, 3, 5, 2, 6, 1, 7, 0)
 
@@ -552,14 +552,26 @@
             pl.when(when())(lambda make=make: make().wait_send())
 
 
-def settle(factor, tg_ref, vg_ref, dw_ref, tg_out, vg_out, dwq_out, dwk_out):
-    tg_out[...] = tg_ref[...]
-    vg_out[...] = vg_ref[...]
+def settle(factor, tg_hbm, vg_hbm, dw_hbm, tg_out, vg_out, dwq_out, dwk_out, tg_ref, vg_ref, dw_ref, sem):
+    dw_in = pltpu.make_async_copy(dw_hbm, dw_ref, sem.at[0])
+    tg_in = pltpu.make_async_copy(tg_hbm, tg_ref, sem.at[1])
+    vg_in = pltpu.make_async_copy(vg_hbm, vg_ref, sem.at[2])
+    tg_go = pltpu.make_async_copy(tg_ref, tg_out, sem.at[3])
+    vg_go = pltpu.make_async_copy(vg_ref, vg_out, sem.at[4])
+    for c in (dw_in, tg_in, vg_in):
+        c.start()
+    tg_in.wait()
+    tg_go.start()
+    vg_in.wait()
+    vg_go.start()
+    dw_in.wait()
     for p in range(8):
         lanes = slice(p * 128, (p + 1) * 128)
         q, k = join(dw_ref[2 * p].astype(F32), dw_ref[2 * p + 1].astype(F32))
         dwq_out[:, lanes] = q * factor
         dwk_out[:, lanes] = k * factor
+    tg_go.wait()
+    vg_go.wait()
 
 
 def body(tokens, query_weight, key_weight, values, lambdas, out_grad):
@@ -599,8 +611,9 @@
         functools.partial(settle, 1.0 / math.sqrt(16 * SEQ)),
         out_shape=(jax.ShapeDtypeStruct((TOK, D), BF16), jax.ShapeDtypeStruct((TOK, COLS), BF16),
                    jax.ShapeDtypeStruct((128, COLS), F32), jax.ShapeDtypeStruct((128, COLS), F32)),
-        in_specs=[vm] * 3,
-        out_specs=(vm,) * 4,
+        in_specs=[pl.BlockSpec(memory_space=pl.ANY)] * 3,
+        out_specs=(pl.BlockSpec(memory_space=pl.ANY),) * 2 + (vm,) * 2,
+        scratch_shapes=[V((TOK, D), BF16), V((TOK, COLS), BF16), V((16, 128, 128), BF16), dma((5,))],
         name="settle",
     )(*raw)
     return tg[None], vg[None], dq, dk

time: 115 us -> 115 us (level)
  no operation moved by 1% of the time
where the time goes in v6:
time: 115 us; the launch traced here: 114 us
  Pallas kernels  114 us (99%)
    pallas_call x1, Pallas kernels, body(): pl.pallas_call(kernel, out_shape=return_shapes, in_specs=[pl.BlockSpec(me...  111 us
    pallas_call x1, Pallas kernels, body(): pl.pallas_call(functools.partial(settle, 1.0 / math.sqrt(16 * SEQ)), out_...  3.2 us

profile of v6, /device:TPU:1, one launch (start us, length us, event | category | flops | bytes accessed | tf_op | source)
XLA Modules:
  0.0 114.5 jit_solution(4218828126097851039)
XLA Ops:
  0.6 110.7 %differential_backward.1 = (bf16[160,2048]{1,0:T(8,128)(2,1)}, bf16[160,1024]{1,0:T(8,128)(2,1)}, bf16[16,128,128]{2,1,0:T(8,128)(2,1)}) custom-call(f32[16]{0:T(128)} %lam_ref.1, bf16[160,2048]{1,0:T(8,128)(2,1)} %bitcast.5, bf16[128,1024]{1,0:T(8,128)(2,1)} %wq_ref.1, bf16[128,1024]{1,0:T(8,128)(2,1)} %wk_ref.1, bf16[160,1024]{1,0:T(8,128)(2,1)} %bitcast.6, ...), custom_call_target="tpu_custom_call" | custom-call | tf_op jit(solution)/shard_map/differential_backward/pallas_call | solution.py:589
  111.3 3.2 %settle.1 = (bf16[160,2048]{1,0:T(8,128)(2,1)}, bf16[160,1024]{1,0:T(8,128)(2,1)}, f32[128,1024]{1,0:T(8,128)}, f32[128,1024]{1,0:T(8,128)}) custom-call(bf16[160,2048]{1,0:T(8,128)(2,1)} %get-tuple-element.11.tg_hbm, bf16[160,1024]{1,0:T(8,128)(2,1)} %get-tuple-element.12.vg_hbm, bf16[16,128,128]{2,1,0:T(8,128)(2,1)} %get-tuple-element.13.dw_hbm), custom_call_target="tpu_custom_call" | custom-call | tf_op jit(solution)/shard_map/settle/pallas_call | solution.py:610
